TPU v7x, 32 devices: a whole 2x2x4 slice. The times are simulated.
32 devices in a mesh: sp: 8 (over z, core), tp: 4 (over y, x).
Axes of the slice: x: 2, y: 2, z: 4, core: 2. Of those that a mesh axis runs over, the one named last changes fastest.
Arguments:
- layer_input: bfloat16 [8, 1024, 2048], P(None, 'sp', 'tp'), may hold values from -6 to 6
- w_key: bfloat16 [2048, 2048], P(None, 'tp'), may hold values from -0.125 to 0.125
- w_value: bfloat16 [2048, 2048], P(None, 'tp'), may hold values from -0.125 to 0.125
- w_gates: bfloat16 [2, 2048, 16], replicated, may hold values from -0.125 to 0.125
- decay_rate: float32 [16], P('tp'), may hold values from 0 to 1, as said below
- beta_bias: float32 [16], P('tp'), may hold values from -5.5 to -3
- log_decay_extra: float32 [8, 16, 1024], P(None, 'tp', 'sp'), may hold values from -2 to 0, as said below
- new_query: bfloat16 [8, 2048], P(None, 'tp'), may hold values from -6 to 6
- read_gain: float32 [128], replicated, may hold values from 0.1 to 1.9
Outputs:
- state_cache: bfloat16 [1024, 2048], P('sp', 'tp')
- first_read: bfloat16 [8, 2048], P(None, 'tp')
Inputs may be any that keep to these rules, and one draw needn't show every extreme that they name: `decay_rate`: a positive rate for each head. `log_decay_extra`: additions that are never positive.
All inputs are finite; a program needn't handle non-finite values.
Results may differ from a plain program's by a relative error of at most 0.0052.
Values may be sent and summed in bfloat16 or wider, within the bound.
A program may use at most 64 MiB of HBM per device.

v0:
```python
import functools

import jax
import jax.numpy as jnp
from jax import lax
from jax.experimental import pallas as pl
from jax.experimental.pallas import tpu as pltpu
from jax.sharding import PartitionSpec as P

DK = 128
DV = 128
EPS = 1e-06
HIGH = lax.Precision.HIGHEST
BF = jnp.bfloat16
F32 = jnp.float32


def dot(left, right, dims=((1,), (0,)), precision=None):
    return lax.dot_general(
        left, right, (dims, ((), ())), precision=precision, preferred_element_type=F32
    )


def kernel(
    n_sp,
    n_tp,
    nh,
    rows,
    x_hbm,
    wk_hbm,
    wv_hbm,
    gates_ref,
    rate_ref,
    bias_ref,
    extra_ref,
    query_ref,
    gain_ref,
    state_out,
    read_out,
    gath,
    w,
    graw,
    level,
    upper,
    maps,
    adds,
    decs,
    pair_maps,
    pair_adds,
    pair_decs,
    joint_decs,
    came,
    sent,
    final,
    landing,
    read_buf,
    read_land,
    query_heads,
    local_sem,
    gsend,
    grecv,
    psend,
    precv,
    csend,
    crecv,
    ssend,
    srecv,
    rsend,
    rrecv,
):
    prompts, seg, depth = x_hbm.shape
    width = nh * DK
    heads = gates_ref.shape[0] // 2
    sp = lax.axis_index("sp")
    tp = lax.axis_index("tp")
    core = lax.rem(sp, 2)
    other = 1 - core
    chip = sp // 2
    last_chip = n_sp // 2 - 1
    share = max(nh // 2, 1)
    mine = core * share
    theirs = other * share
    has_mine = mine < nh
    has_theirs = theirs < nh
    sources = [k for k in range(2) if k * share < nh]
    chunks = DK // rows
    relay = n_tp == 4

    x_copy = pltpu.make_async_copy(x_hbm, gath.at[tp], local_sem.at[0])
    x_copy.start()
    wk_copy = pltpu.make_async_copy(wk_hbm, w.at[:, pl.ds(0, width)], local_sem.at[1])
    wv_copy = pltpu.make_async_copy(wv_hbm, w.at[:, pl.ds(width, nh * DV)], local_sem.at[2])
    wk_copy.start()
    wv_copy.start()

    barrier = pltpu.get_barrier_semaphore()

    def greet_tp(step, carry):
        pl.semaphore_signal(barrier, inc=1, device_id={"tp": lax.rem(tp + step, n_tp)})
        return carry

    def greet_sp(step, carry):
        pl.semaphore_signal(barrier, inc=1, device_id={"sp": lax.rem(sp + step, n_sp)})
        return carry

    lax.fori_loop(1, n_tp, greet_tp, 0)
    lax.fori_loop(1, n_sp, greet_sp, 0)
    r_id = lax.broadcasted_iota(jnp.int32, (seg, seg), 0)
    c_id = lax.broadcasted_iota(jnp.int32, (seg, seg), 1)
    lev = jnp.zeros((seg, seg), jnp.int32)
    k = 1
    while (1 << k) < seg:
        lev = jnp.where((r_id >> k) != (c_id >> k), k, lev)
        k += 1
    levels = k
    level[...] = jnp.where(r_id > c_id, lev, -1)
    upper[...] = jnp.where(r_id <= c_id, 1.0, 0.0).astype(F32)
    graw[...] = jnp.zeros_like(graw)
    pl.semaphore_wait(barrier, n_tp - 1 + n_sp - 1)
    x_copy.wait()

    xn = tp + 1 - 2 * lax.rem(tp, 2)
    yn = tp + 2 - 4 * (tp // 2)
    half = seg // 2

    def direct(p, way):
        target = xn if way == 0 else yn
        return pltpu.make_async_remote_copy(
            src_ref=gath.at[tp, p],
            dst_ref=gath.at[tp, p],
            send_sem=gsend.at[way, p],
            recv_sem=grecv.at[way, p],
            device_id={"tp": target},
        )

    def passed(p, way):
        source = xn if way == 0 else yn
        target = yn if way == 0 else xn
        part = pl.ds(way * half, half)
        return pltpu.make_async_remote_copy(
            src_ref=gath.at[source, p, part],
            dst_ref=gath.at[source, p, part],
            send_sem=gsend.at[2 + way, p],
            recv_sem=grecv.at[2 + way, p],
            device_id={"tp": target},
        )

    def plain(p, step):
        return pltpu.make_async_remote_copy(
            src_ref=gath.at[tp, p],
            dst_ref=gath.at[tp, p],
            send_sem=gsend.at[step, p],
            recv_sem=grecv.at[step, p],
            device_id={"tp": lax.rem(tp + step, n_tp)},
        )

    def start_direct(p):
        direct(p, 0).start()
        direct(p, 1).start()

    def pass_on(p):
        direct(p, 0).wait_recv()
        passed(p, 0).start()
        direct(p, 1).wait_recv()
        passed(p, 1).start()

    early = min(2, prompts)
    ahead = min(1, prompts)
    if relay:
        for p in range(early):
            start_direct(p)
        for p in range(ahead):
            pass_on(p)
            if early + p < prompts:
                start_direct(early + p)
    else:

        def start_plain(index, carry):
            plain(index // (n_tp - 1), lax.rem(index, n_tp - 1) + 1).start()
            return carry

        lax.fori_loop(0, prompts * (n_tp - 1), start_plain, 0)
    wk_copy.wait()
    wv_copy.wait()

    def pair_copies(p):
        pairs = (
            (maps.at[p, pl.ds(theirs, share)], pair_maps.at[p]),
            (adds.at[p, pl.ds(theirs, share)], pair_adds.at[p]),
            (decs.at[p], pair_decs.at[p]),
        )
        return [
            pltpu.make_async_remote_copy(
                src_ref=source,
                dst_ref=target,
                send_sem=psend.at[i, p],
                recv_sem=precv.at[i, p],
                device_id={"sp": sp + 1 - 2 * core},
            )
            for i, (source, target) in enumerate(pairs)
        ]

    def chain_copy(p, j):
        return pltpu.make_async_remote_copy(
            src_ref=sent.at[p, j],
            dst_ref=came.at[p, j],
            send_sem=csend.at[p, j],
            recv_sem=crecv.at[p, j],
            device_id={"sp": lax.rem(sp + 2, n_sp)},
        )

    def state_copy(p, c, slot):
        return pltpu.make_async_remote_copy(
            src_ref=final.at[p, :, pl.ds(c * rows, rows)],
            dst_ref=landing.at[pl.ds(slot * share, share)],
            send_sem=ssend.at[p, c],
            recv_sem=srecv.at[slot],
            device_id={"sp": p * chunks + c},
        )

    def read_copy(target, slot):
        return pltpu.make_async_remote_copy(
            src_ref=read_buf,
            dst_ref=read_land.at[pl.ds(slot * share, share)],
            send_sem=rsend.at[target],
            recv_sem=rrecv.at[slot],
            device_id={"sp": target},
        )

    first_head = tp * nh
    pad = 8
    row_id = lax.broadcasted_iota(jnp.int32, (pad, seg), 0)

    def work(p):
        x = jnp.concatenate([gath[s, p] for s in range(n_tp)], axis=1)
        pre = dot(x, w[...])
        gt = dot(gates_ref[...], x, ((1,), (1,)))
        graw[0, pl.ds(0, heads)] = gt[:heads]
        graw[1, pl.ds(0, heads)] = gt[heads:]
        gd = graw[0, pl.ds(first_head, pad)]
        gb = graw[1, pl.ds(first_head, pad)]
        rate = jnp.zeros((pad, seg), F32)
        bias = jnp.zeros((pad, seg), F32)
        for h in range(nh):
            rate = jnp.where(row_id == h, rate_ref[h], rate)
            bias = jnp.where(row_id == h, bias_ref[h], bias)
        extra = jnp.concatenate([extra_ref[p], jnp.zeros((pad - nh, seg), F32)], axis=0)
        soft = jnp.maximum(gd, 0.0) + jnp.log1p(jnp.exp(-jnp.abs(gd)))
        log_decay = extra - rate * soft
        beta = jax.nn.sigmoid(gb + bias)
        run = dot(log_decay, upper[...], precision=HIGH)
        end = run[:, seg - 1 : seg]
        decs[p] = jnp.broadcast_to(jnp.exp(end), (pad, DV))
        cols = jnp.concatenate(
            [run, beta, beta * jnp.exp(run), jnp.exp(end - run)], axis=0
        ).T
        act = pre * jax.nn.sigmoid(pre)
        lev = level[...]
        strict = lev >= 0
        eye = jnp.where(
            lax.broadcasted_iota(jnp.int32, (seg, seg), 0)
            == lax.broadcasted_iota(jnp.int32, (seg, seg), 1),
            1.0,
            0.0,
        ).astype(F32)
        keys, lower, inv = [], [], []
        for h in range(nh):
            raw = act[:, h * DK : (h + 1) * DK]
            key = raw * lax.rsqrt(jnp.sum(raw * raw, axis=-1, keepdims=True) + EPS)
            kb = key.astype(BF)
            gram = dot(kb, kb, ((1,), (1,)))
            spread = cols[:, h : h + 1] - run[h : h + 1, :]
            weight = jnp.exp(jnp.where(strict, spread, 0.0))
            low = jnp.where(strict, gram * weight * cols[:, pad + h : pad + h + 1], 0.0)
            keys.append(key)
            lower.append(low)
            inv.append(jnp.where(lev == 0, -low, 0.0))
        for step in range(1, levels):
            cuts = [jnp.where(lev == step, low, 0.0) for low in lower]
            full = [(eye + part).astype(BF) for part in inv]
            mids = [dot(cut.astype(BF), f) for cut, f in zip(cuts, full)]
            inv = [
                part - dot(f, mid.astype(BF)) for part, f, mid in zip(inv, full, mids)
            ]
        for h in range(nh):
            value = act[:, width + h * DV : width + (h + 1) * DV]
            side = jnp.concatenate(
                [
                    value * cols[:, pad + h : pad + h + 1],
                    keys[h] * cols[:, 2 * pad + h : 2 * pad + h + 1],
                ],
                axis=1,
            )
            solved = side + dot(inv[h].astype(BF), side.astype(BF))
            late = keys[h] * cols[:, 3 * pad + h : 3 * pad + h + 1]
            late_top = late.astype(BF)
            late_rest = (late - late_top.astype(F32)).astype(BF)
            top = solved.astype(BF)
            rest = (solved[:, :DV] - top[:, :DV].astype(F32)).astype(BF)
            tall = ((0,), (0,))
            both = dot(late_top, top, tall)
            adds[p, h] = (
                both[:, :DV] + dot(late_top, rest, tall) + dot(late_rest, top[:, :DV], tall)
            )
            maps[p, h] = both[:, DV:].astype(BF)

    def unite(p):
        def merge(j, early, late, early_dec, late_dec):
            h = mine + j
            map_0, add_0 = early[0][...], early[1][...]
            map_1, add_1 = late[0][...], late[1][...]
            dec_0 = early_dec[p, pl.ds(h, 1)]
            dec_1 = late_dec[p, pl.ds(h, 1)]
            turn = dot(map_1, jnp.concatenate([map_0, add_0.astype(BF)], axis=1))
            maps[p, h] = (
                dec_1 * map_0.astype(F32) + dec_0 * map_1.astype(F32) - turn[:, :DK]
            ).astype(BF)
            adds[p, h] = dec_1 * add_0 + add_1 - turn[:, DK:]

        @pl.when(has_mine)
        def _():
            for copy in pair_copies(p):
                copy.wait_recv()
            joint_decs[p] = decs[p] * pair_decs[p]
            for first in range(2):

                @pl.when(core == first)
                def _():
                    for j in range(share):
                        own = (maps.at[p, mine + j], adds.at[p, mine + j])
                        got = (pair_maps.at[p, j], pair_adds.at[p, j])
                        if first == 0:
                            merge(j, own, got, decs, pair_decs)
                        else:
                            merge(j, got, own, pair_decs, decs)

    def advance(p):
        @pl.when(chip == 0)
        def _():
            for j in range(share):
                sent[p, j] = adds[p, mine + j].astype(BF)
                chain_copy(p, j).start()

        def moved(j):
            chain_copy(p, j).wait_recv()
            state = came[p, j]
            h = mine + j
            return (
                joint_decs[p, pl.ds(h, 1)] * state.astype(F32)
                + adds[p, h]
                - dot(maps[p, h], state)
            )

        @pl.when(jnp.logical_and(chip > 0, chip < last_chip))
        def _():
            for j in range(share):
                sent[p, j] = moved(j).astype(BF)
                chain_copy(p, j).start()

        @pl.when(chip == last_chip)
        def _():
            for j in range(share):
                state = moved(j).astype(BF)
                final[p, j] = state
                raw = dot(query_heads[mine + j], state)
                norm = (
                    raw
                    * lax.rsqrt(jnp.mean(raw * raw, axis=-1, keepdims=True) + EPS)
                    * gain_ref[...]
                )
                at_p = lax.broadcasted_iota(jnp.int32, norm.shape, 0) == p
                read_buf[j] = jnp.where(at_p, norm, read_buf[j])
            for c in range(chunks):
                owner = p * chunks + c

                @pl.when(owner != sp)
                def _():
                    state_copy(p, c, core).start()

                @pl.when(owner == sp)
                def _():
                    for j in range(share):
                        landing[mine + j] = final[p, j, c * rows : (c + 1) * rows]

    ending = jnp.logical_and(chip == last_chip, has_mine)

    @pl.when(ending)
    def _():
        read_buf[...] = jnp.zeros_like(read_buf)
        for h in range(nh):
            query_heads[h] = query_ref[:, h * DK : (h + 1) * DK]

    lag = 1 + chip

    def body(it, carry):
        if relay:

            @pl.when(it + ahead < prompts)
            def _():
                pass_on(it + ahead)

            @pl.when(it + ahead + early < prompts)
            def _():
                start_direct(it + ahead + early)

        @pl.when(it < prompts)
        def _():
            if relay:
                passed(it, 0).wait_recv()
                passed(it, 1).wait_recv()
            else:

                def take(step, carry):
                    plain(it, step).wait_recv()
                    return carry

                lax.fori_loop(1, n_tp, take, 0)
            work(it)

            @pl.when(has_theirs)
            def _():
                for copy in pair_copies(it):
                    copy.start()

        @pl.when(jnp.logical_and(it >= 1, it < prompts + 1))
        def _():
            unite(it - 1)

        moving = jnp.logical_and(it >= lag, it < prompts + lag)

        @pl.when(jnp.logical_and(moving, has_mine))
        def _():
            advance(it - lag)

        return carry

    lax.fori_loop(0, prompts + last_chip + 1, body, 0)

    @pl.when(ending)
    def _():
        def tell(target, carry):
            @pl.when(target != sp)
            def _():
                read_copy(target, core).start()

            return carry

        lax.fori_loop(0, n_sp, tell, 0)
        for j in range(share):
            read_land[mine + j] = read_buf[j]

    for k in sources:

        @pl.when(sp != 2 * last_chip + k)
        def _():
            state_copy(0, 0, k).wait_recv()
            read_copy(0, k).wait_recv()

    for h in range(nh):
        state_out[:, h * DV : (h + 1) * DV] = landing[h]
        read_out[:, h * DV : (h + 1) * DV] = read_land[h].astype(BF)

    @pl.when(ending)
    def _():
        def told(target, carry):
            @pl.when(target != sp)
            def _():
                read_copy(target, core).wait_send()
                state_copy(target // chunks, lax.rem(target, chunks), core).wait_send()

            return carry

        lax.fori_loop(0, n_sp, told, 0)

    @pl.when(jnp.logical_and(chip < last_chip, has_mine))
    def _():
        def left(index, carry):
            chain_copy(index // share, lax.rem(index, share)).wait_send()
            return carry

        lax.fori_loop(0, prompts * share, left, 0)

    @pl.when(has_theirs)
    def _():
        def lent(index, carry):
            for copy in pair_copies(index):
                copy.wait_send()
            return carry

        lax.fori_loop(0, prompts, lent, 0)

    def freed(index, carry):
        if relay:
            direct(index, 0).wait_send()
            direct(index, 1).wait_send()
            passed(index, 0).wait_send()
            passed(index, 1).wait_send()
        else:
            for step in range(1, n_tp):
                plain(index, step).wait_send()
        return carry

    lax.fori_loop(0, prompts, freed, 0)


def shards(
    n_sp,
    n_tp,
    layer_input,
    w_key,
    w_value,
    w_gates,
    decay_rate,
    beta_bias,
    log_decay_extra,
    new_query,
    read_gain,
):
    prompts, seg, depth = layer_input.shape
    whole_depth, width = w_key.shape
    nh = width // DK
    heads = w_gates.shape[2]
    rows = prompts * DK // n_sp
    share = max(nh // 2, 1)
    gates = jnp.swapaxes(w_gates, 1, 2).reshape(2 * heads, whole_depth)
    vmem = pl.BlockSpec(memory_space=pltpu.VMEM)
    smem = pl.BlockSpec(memory_space=pltpu.SMEM)
    hbm = pl.BlockSpec(memory_space=pl.ANY)
    dma = pltpu.SemaphoreType.DMA
    return pl.pallas_call(
        functools.partial(kernel, n_sp, n_tp, nh, rows),
        out_shape=(
            jax.ShapeDtypeStruct((rows, nh * DV), BF),
            jax.ShapeDtypeStruct((prompts, nh * DV), BF),
        ),
        in_specs=[hbm, hbm, hbm, vmem, smem, smem, vmem, vmem, vmem],
        out_specs=(vmem, vmem),
        scratch_shapes=[
            pltpu.VMEM((n_tp, prompts, seg, depth), BF),
            pltpu.VMEM((whole_depth, nh * (DK + DV)), BF),
            pltpu.VMEM((2, heads + 8, seg), F32),
            pltpu.VMEM((seg, seg), jnp.int32),
            pltpu.VMEM((seg, seg), F32),
            pltpu.VMEM((prompts, nh, DK, DK), BF),
            pltpu.VMEM((prompts, nh, DK, DV), F32),
            pltpu.VMEM((prompts, 8, DV), F32),
            pltpu.VMEM((prompts, share, DK, DK), BF),
            pltpu.VMEM((prompts, share, DK, DV), F32),
            pltpu.VMEM((prompts, 8, DV), F32),
            pltpu.VMEM((prompts, 8, DV), F32),
            pltpu.VMEM((prompts, share, DK, DV), BF),
            pltpu.VMEM((prompts, share, DK, DV), BF),
            pltpu.VMEM((prompts, share, DK, DV), BF),
            pltpu.VMEM((nh, rows, DV), BF),
            pltpu.VMEM((share, prompts, DV), F32),
            pltpu.VMEM((nh, prompts, DV), F32),
            pltpu.VMEM((nh, prompts, DK), BF),
            dma((3,)),
            dma((max(n_tp, 4), prompts)),
            dma((max(n_tp, 4), prompts)),
            dma((3, prompts)),
            dma((3, prompts)),
            dma((prompts, share)),
            dma((prompts, share)),
            dma((prompts, DK // rows)),
            dma((2,)),
            dma((n_sp,)),
            dma((2,)),
        ],
        compiler_params=pltpu.CompilerParams(
            collective_id=0, has_side_effects=True, vmem_limit_bytes=56 * 1024 * 1024
        ),
    )(
        layer_input,
        w_key,
        w_value,
        gates,
        decay_rate,
        beta_bias,
        log_decay_extra,
        new_query,
        read_gain.reshape(1, DV),
    )


def solution(mesh):
    return jax.shard_map(
        functools.partial(shards, mesh.shape["sp"], mesh.shape["tp"]),
        mesh=mesh,
        in_specs=(
            P(None, "sp", "tp"),
            P(None, "tp"),
            P(None, "tp"),
            P(),
            P("tp"),
            P("tp"),
            P(None, "tp", "sp"),
            P(None, "tp"),
            P(),
        ),
        out_specs=(P("sp", "tp"), P(None, "tp")),
        check_vma=False,
    )
```

profile of v0, /device:TPU:0, one launch (start us, length us, event | category | flops | bytes accessed | tf_op | source)
XLA Modules:
  0.0 71.9 jit_solution(16182332937237379052)
XLA Ops:
  0.6 68.4 %shard_map.104 = (bf16[128,512]{1,0:T(8,128)(2,1)}, bf16[8,512]{1,0:T(8,128)(2,1)}) custom-call(bf16[8,128,512]{2,1,0:T(8,128)(2,1)} %x_hbm.1, bf16[2048,512]{1,0:T(8,128)(2,1)} %wk_hbm.1, bf16[2048,512]{1,0:T(8,128)(2,1)} %wv_hbm.1, bf16[32,2048]{1,0:T(8,128)(2,1)} %bitcast.4, f32[4]{0:T(128)} %rate_ref.1, f32[4]{0:T(128)} %bias_ref.1, ...), custom_call_target="tpu_custom_call" | custom-call | tf_op jit(solution)/shard_map/pallas_call | solution.py:530
  69.0 1.6 %copy.13 = bf16[128,512]{1,0:T(8,128)(2,1)} copy(bf16[128,512]{1,0:T(8,128)(2,1)} %get-tuple-element.4) | data formatting | bytes 262144
  70.6 1.3 %copy.14 = bf16[8,512]{1,0:T(8,128)(2,1)} copy(bf16[8,512]{1,0:T(8,128)(2,1)} %get-tuple-element.5) | data formatting | bytes 16384
where the time goes:
time: 72.1 us; the launch traced here: 71.9 us
  Pallas kernels  68.4 us (95%)
  local copies, waits for them, and re-layouts  2.86 us (4%)
    pallas_call x1, Pallas kernels, shards(): pl.pallas_call(functools.partial(kernel, n_sp, n_tp, nh, rows), out_shape...  68.4 us
    unnamed x2, local copies, waits for them, and re-layouts  2.86 us

commit v1 on v0

--- a/solution.py
+++ b/solution.py
@@ -503,6 +503,556 @@
     lax.fori_loop(0, prompts, freed, 0)
 
 
+def near(
+    n_sp,
+    n_tp,
+    nh,
+    x_hbm,
+    wk_hbm,
+    wv_hbm,
+    gates_ref,
+    rate_ref,
+    bias_ref,
+    extra_ref,
+    query_ref,
+    gain_ref,
+    state_out,
+    read_out,
+    gath,
+    w,
+    gall,
+    gsel,
+    fixed,
+    level,
+    upper,
+    acc,
+    gacc,
+    maps,
+    adds,
+    decs,
+    up_out,
+    up_in,
+    map_out,
+    map_in,
+    add_out,
+    add_in,
+    dec_out,
+    dec_in,
+    query,
+    read_buf,
+    read_land,
+    local_sem,
+    gsend,
+    grecv,
+    usend,
+    urecv,
+    dsend,
+    drecv,
+    rsend,
+    rrecv,
+):
+    prompts, seg, depth = x_hbm.shape
+    width = nh * DK
+    heads = gates_ref.shape[0] // 2
+    pad = 8
+    last = n_sp - 1
+    sp = lax.axis_index("sp")
+    tp = lax.axis_index("tp")
+    core = lax.rem(sp, 2)
+
+    x_copy = pltpu.make_async_copy(x_hbm, gath.at[tp], local_sem.at[0])
+    x_copy.start()
+    wk_copy = pltpu.make_async_copy(wk_hbm, w.at[:, pl.ds(0, width)], local_sem.at[1])
+    wv_copy = pltpu.make_async_copy(wv_hbm, w.at[:, pl.ds(width, nh * DV)], local_sem.at[2])
+    wk_copy.start()
+    wv_copy.start()
+
+    barrier = pltpu.get_barrier_semaphore()
+    xn = tp + 1 - 2 * lax.rem(tp, 2)
+    yn = tp + 2 - 4 * (tp // 2)
+    far = n_tp - 1 - tp
+
+    pl.semaphore_signal(barrier, inc=1, device_id={"tp": xn})
+    pl.semaphore_signal(barrier, inc=1, device_id={"tp": yn})
+
+    def greet_sp(step, carry):
+        pl.semaphore_signal(barrier, inc=1, device_id={"sp": lax.rem(sp + step, n_sp)})
+        return carry
+
+    lax.fori_loop(1, n_sp, greet_sp, 0)
+
+    r_id = lax.broadcasted_iota(jnp.int32, (seg, seg), 0)
+    c_id = lax.broadcasted_iota(jnp.int32, (seg, seg), 1)
+    lev = jnp.zeros((seg, seg), jnp.int32)
+    k = 1
+    while (1 << k) < seg:
+        lev = jnp.where((r_id >> k) != (c_id >> k), k, lev)
+        k += 1
+    levels = k
+    level[...] = jnp.where(r_id > c_id, lev, -1)
+    upper[...] = jnp.where(r_id <= c_id, 1.0, 0.0).astype(BF)
+    groups = [(k, min(k + 3, levels)) for k in range(1, levels, 3)]
+
+    row_id = lax.broadcasted_iota(jnp.int32, (pad, seg), 0)
+    rate = jnp.zeros((pad, seg), F32)
+    bias = jnp.zeros((pad, seg), F32)
+    for h in range(nh):
+        rate = jnp.where(row_id == h, rate_ref[h], rate)
+        bias = jnp.where(row_id == h, bias_ref[h], bias)
+    fixed[0] = rate
+    fixed[1] = bias
+    for at in range(n_tp * depth // 128):
+        part = gates_ref[:, at * 128 : (at + 1) * 128].astype(F32)
+        gall[at, pl.ds(0, heads)] = part[:heads]
+        gall[at, pl.ds(heads, heads)] = part[heads:]
+        gall[at, pl.ds(2 * heads, pad)] = jnp.zeros((pad, 128), F32)
+        picked = [gall[at, pl.ds(tp * nh + k * heads, pad)] for k in range(2)]
+        gsel[:, at * 128 : (at + 1) * 128] = jnp.concatenate(picked, axis=0).astype(BF)
+    every = query_ref[...].astype(F32)
+    mine = lax.broadcasted_iota(jnp.int32, every.shape, 0) == sp
+    asked = jnp.sum(jnp.where(mine, every, 0.0), axis=0, keepdims=True)
+    for h in range(nh):
+        query[h] = jnp.broadcast_to(asked[:, h * DK : (h + 1) * DK], (pad, DK))
+    read_buf[...] = jnp.zeros_like(read_buf)
+
+    @pl.when(core == 0)
+    def _():
+        up_in[:, 1] = jnp.zeros((n_sp - 1, nh, DK, DV), BF)
+
+    @pl.when(core == 1)
+    def _():
+        add_in[:, 1] = jnp.zeros((n_sp - 1, nh, DK, DV), BF)
+
+    pl.semaphore_wait(barrier, 2 + n_sp - 1)
+    x_copy.wait()
+
+    half = seg // 2
+
+    def prompt_at(t):
+        rev = last - t
+        p = 0
+        k = 1
+        while k < n_sp:
+            p = p + k * lax.rem(sp // k + rev // k, 2)
+            k *= 2
+        return p
+
+    def direct(t, way):
+        p = prompt_at(t)
+        return pltpu.make_async_remote_copy(
+            src_ref=gath.at[tp, p],
+            dst_ref=gath.at[tp, p],
+            send_sem=gsend.at[way, t],
+            recv_sem=grecv.at[way, t],
+            device_id={"tp": xn if way == 0 else yn},
+        )
+
+    def passed(t, way):
+        p = prompt_at(t)
+        source = xn if way == 0 else yn
+        part = pl.ds(way * half, half)
+        return pltpu.make_async_remote_copy(
+            src_ref=gath.at[source, p, part],
+            dst_ref=gath.at[source, p, part],
+            send_sem=gsend.at[2 + way, t],
+            recv_sem=grecv.at[2 + way, t],
+            device_id={"tp": yn if way == 0 else xn},
+        )
+
+    def start_direct(t):
+        direct(t, 0).start()
+        direct(t, 1).start()
+
+    def pass_on(t):
+        direct(t, 0).wait_recv()
+        passed(t, 0).start()
+        direct(t, 1).wait_recv()
+        passed(t, 1).start()
+
+    def up_copy(t, part):
+        return pltpu.make_async_remote_copy(
+            src_ref=up_out.at[t, part],
+            dst_ref=up_in.at[t, part],
+            send_sem=usend.at[part, t],
+            recv_sem=urecv.at[part, t],
+            device_id={"sp": sp + 1},
+        )
+
+    def down_copy(t, part):
+        pairs = (
+            (map_out.at[t], map_in.at[t]),
+            (add_out.at[t, 0], add_in.at[t, 0]),
+            (dec_out.at[t], dec_in.at[t]),
+            (add_out.at[t, 1], add_in.at[t, 1]),
+        )
+        return pltpu.make_async_remote_copy(
+            src_ref=pairs[part][0],
+            dst_ref=pairs[part][1],
+            send_sem=dsend.at[part, t],
+            recv_sem=drecv.at[part, t],
+            device_id={"sp": sp - 1},
+        )
+
+    def read_copy(target, source):
+        return pltpu.make_async_remote_copy(
+            src_ref=read_buf,
+            dst_ref=read_land.at[source],
+            send_sem=rsend.at[target],
+            recv_sem=rrecv.at[source],
+            device_id={"sp": target},
+        )
+
+    def band(source):
+        return pl.ds(pl.multiple_of(source * depth, depth), depth)
+
+    tile = DK + DV
+    near_by = (tp, xn, yn)
+
+    def ahead(t):
+        p = prompt_at(t)
+        slot = lax.rem(t, 2)
+        x = jnp.concatenate([gath[s, p] for s in near_by], axis=1)
+
+        def gate_piece():
+            g = jnp.concatenate([gsel[:, band(s)] for s in near_by], axis=1)
+            gacc[slot] = dot(g, x, ((1,), (1,)))
+
+        def piece(at):
+            def go():
+                cols = pl.ds(at * tile, tile)
+                side = jnp.concatenate([w[band(s), cols] for s in near_by], axis=0)
+                acc[slot, :, cols] = dot(x, side)
+
+            return go
+
+        return [gate_piece] + [piece(at) for at in range(2 * width // tile)]
+
+    def work(t, pieces):
+        pieces = list(pieces)
+
+        def fill():
+            if pieces:
+                pieces.pop(0)()
+
+        p = prompt_at(t)
+        slot = lax.rem(t, 2)
+        x = gath[far, p]
+        gt = gacc[slot] + dot(gsel[:, band(far)], x, ((1,), (1,)))
+        key_pre = acc[slot, :, :width] + dot(x, w[band(far), :width])
+        value_pre = acc[slot, :, width:] + dot(x, w[band(far), width:])
+        gd = gt[:pad]
+        gb = gt[pad:]
+        extra = jnp.concatenate([extra_ref[p], jnp.zeros((pad - nh, seg), F32)], axis=0)
+        soft = jnp.maximum(gd, 0.0) + jnp.log1p(jnp.exp(-jnp.abs(gd)))
+        log_decay = extra - fixed[0] * soft
+        beta = jax.nn.sigmoid(gb + fixed[1])
+        high = log_decay.astype(BF).astype(F32)
+        rest = log_decay - high
+        mid = rest.astype(BF).astype(F32)
+        split = jnp.concatenate([high, mid, rest - mid, jnp.zeros_like(high)], axis=0)
+        sums = dot(split.astype(BF), upper[...])
+        run = sums[:pad] + sums[pad : 2 * pad] + sums[2 * pad : 3 * pad]
+        end = run[:, seg - 1 : seg]
+        decs[p] = jnp.broadcast_to(jnp.exp(end), (pad, DV))
+        cols = jnp.concatenate(
+            [run, beta, beta * jnp.exp(run), jnp.exp(end - run)], axis=0
+        ).T
+        lev = level[...]
+        strict = lev >= 0
+        eye = jnp.where(
+            lax.broadcasted_iota(jnp.int32, (seg, seg), 0)
+            == lax.broadcasted_iota(jnp.int32, (seg, seg), 1),
+            1.0,
+            0.0,
+        ).astype(F32)
+        hs = range(nh)
+        keys, grams = [], []
+        for h in hs:
+            pre = key_pre[:, h * DK : (h + 1) * DK]
+            raw = pre * jax.nn.sigmoid(pre)
+            key = raw * lax.rsqrt(jnp.sum(raw * raw, axis=-1, keepdims=True) + EPS)
+            kb = key.astype(BF)
+            keys.append(key)
+            grams.append(dot(kb, kb, ((1,), (1,))))
+        fill()
+        fill()
+        lower, inv = [], []
+        for h in hs:
+            spread = cols[:, h : h + 1] - run[h : h + 1, :]
+            weight = jnp.exp(jnp.where(strict, spread, 0.0))
+            low = jnp.where(strict, grams[h] * weight * cols[:, pad + h : pad + h + 1], 0.0)
+            lower.append(low)
+            inv.append(eye - jnp.where(lev == 0, low, 0.0))
+
+        def merge(first, until):
+            inside = jnp.logical_and(lev >= first, lev < until)
+            cuts = [jnp.where(inside, low, 0.0).astype(BF) for low in lower]
+            return [dot(f.astype(BF), cut).astype(BF) for f, cut in zip(inv, cuts)]
+
+        for first, until in groups[:-1]:
+            steps = merge(first, until)
+            fill()
+            inv = [f - dot(e, f.astype(BF)) for e, f in zip(steps, inv)]
+            for _ in range(first + 1, until):
+                steps = [dot(e, e).astype(BF) for e in steps]
+                fill()
+                inv = [f + dot(e, f.astype(BF)) for e, f in zip(steps, inv)]
+        sides = []
+        for h in hs:
+            pre = value_pre[:, h * DV : (h + 1) * DV]
+            value = pre * jax.nn.sigmoid(pre)
+            sides.append(
+                jnp.concatenate(
+                    [
+                        value * cols[:, pad + h : pad + h + 1],
+                        keys[h] * cols[:, 2 * pad + h : 2 * pad + h + 1],
+                    ],
+                    axis=1,
+                )
+            )
+        first, until = groups[-1]
+        steps = merge(first, until)
+        sides = [
+            side + dot((f - eye).astype(BF), side.astype(BF)) for f, side in zip(inv, sides)
+        ]
+        fill()
+        sides = [side - dot(e, side.astype(BF)) for e, side in zip(steps, sides)]
+        for _ in range(first + 1, until):
+            steps = [dot(e, e).astype(BF) for e in steps]
+            fill()
+            sides = [side + dot(e, side.astype(BF)) for e, side in zip(steps, sides)]
+        while pieces:
+            fill()
+        tall = ((0,), (0,))
+        for h in hs:
+            late = keys[h] * cols[:, 3 * pad + h : 3 * pad + h + 1]
+            late_top = late.astype(BF)
+            late_rest = (late - late_top.astype(F32)).astype(BF)
+            top = sides[h].astype(BF)
+            rest = (sides[h][:, :DV] - top[:, :DV].astype(F32)).astype(BF)
+            both = dot(late_top, top, tall)
+            adds[p, h] = (
+                both[:, :DV] + dot(late_top, rest, tall) + dot(late_rest, top[:, :DV], tall)
+            )
+            maps[p, h] = both[:, DV:].astype(BF)
+
+    def moved(at, p, h):
+        top = up_in[at, 0, h]
+        state = top.astype(F32) + up_in[at, 1, h].astype(F32)
+        return decs[p, pl.ds(h, 1)] * state + adds[p, h] - dot(maps[p, h], top)
+
+    def go_up(t, p, fresh):
+        for h in range(nh):
+            state = adds[p, h] if fresh else moved(t - 1, p, h)
+            top = state.astype(BF)
+            up_out[t, 0, h] = top
+            up_out[t, 1, h] = (state - top.astype(F32)).astype(BF)
+
+    def go_down(t, p, fresh):
+        for h in range(nh):
+            if fresh:
+                total = adds[p, h]
+                map_out[t, h] = maps[p, h]
+            else:
+                own = decs[p, pl.ds(h, 1)]
+                later = dec_in[t - 1, pl.ds(h, 1)]
+                late = map_in[t - 1, h]
+                early = maps[p, h]
+                add = adds[p, h]
+                turn = dot(late, jnp.concatenate([early, add.astype(BF)], axis=1))
+                total = (
+                    later * add
+                    + add_in[t - 1, 0, h].astype(F32)
+                    + add_in[t - 1, 1, h].astype(F32)
+                    - turn[:, DK:]
+                )
+                map_out[t, h] = (
+                    later * early.astype(F32) + own * late.astype(F32) - turn[:, :DK]
+                ).astype(BF)
+            top = total.astype(BF)
+            add_out[t, 0, h] = top
+            add_out[t, 1, h] = (total - top.astype(F32)).astype(BF)
+        dec_out[t] = decs[p] if fresh else decs[p] * dec_in[t - 1]
+
+    def wait_up(t):
+        up_copy(t, 0).wait_recv()
+
+        @pl.when(core == 1)
+        def _():
+            up_copy(t, 1).wait_recv()
+
+    def wait_down(t):
+        for part in range(3):
+            down_copy(t, part).wait_recv()
+
+        @pl.when(core == 0)
+        def _():
+            down_copy(t, 3).wait_recv()
+
+    def chain(t):
+        rev = last - t
+
+        @pl.when(sp + rev <= last)
+        def _():
+            @pl.when(sp == 0)
+            def _():
+                go_up(t, rev, True)
+
+            @pl.when(sp > 0)
+            def _():
+                wait_up(t - 1)
+                go_up(t, sp + rev, False)
+
+            up_copy(t, 0).start()
+
+            @pl.when(core == 0)
+            def _():
+                up_copy(t, 1).start()
+
+        @pl.when(sp >= rev)
+        def _():
+            @pl.when(sp == last)
+            def _():
+                go_down(t, last - rev, True)
+
+            @pl.when(sp < last)
+            def _():
+                wait_down(t - 1)
+                go_down(t, sp - rev, False)
+
+            for part in range(3):
+                down_copy(t, part).start()
+
+            @pl.when(core == 1)
+            def _():
+                down_copy(t, 3).start()
+
+    def close(below, above):
+        at = last - 1
+        for h in range(nh):
+            state = moved(at, sp, h) if below else adds[sp, h]
+            if above:
+                state = (
+                    dec_in[at, pl.ds(h, 1)] * state
+                    + add_in[at, 0, h].astype(F32)
+                    + add_in[at, 1, h].astype(F32)
+                    - dot(map_in[at, h], state.astype(BF))
+                )
+            cached = state.astype(BF)
+            state_out[:, h * DV : (h + 1) * DV] = cached
+            raw = dot(query[h].astype(BF), cached)
+            norm = (
+                raw
+                * lax.rsqrt(jnp.mean(raw * raw, axis=-1, keepdims=True) + EPS)
+                * gain_ref[...]
+            )
+            read_buf[pl.ds(h, 1)] = norm[:1]
+
+    early = min(2, prompts)
+    for t in range(early):
+        start_direct(t)
+    pass_on(0)
+    if early < prompts:
+        start_direct(early)
+    wk_copy.wait()
+    wv_copy.wait()
+    for go in ahead(0):
+        go()
+
+    def body(t, carry):
+        pass_on(t + 1)
+
+        @pl.when(t + 1 + early < prompts)
+        def _():
+            start_direct(t + 1 + early)
+
+        passed(t, 0).wait_recv()
+        passed(t, 1).wait_recv()
+        work(t, ahead(t + 1))
+        chain(t)
+        return carry
+
+    lax.fori_loop(0, last, body, 0)
+    passed(last, 0).wait_recv()
+    passed(last, 1).wait_recv()
+    work(last, [])
+
+    @pl.when(sp > 0)
+    def _():
+        wait_up(last - 1)
+
+    @pl.when(sp < last)
+    def _():
+        wait_down(last - 1)
+
+    @pl.when(sp == 0)
+    def _():
+        close(False, True)
+
+    @pl.when(jnp.logical_and(sp > 0, sp < last))
+    def _():
+        close(True, True)
+
+    @pl.when(sp == last)
+    def _():
+        close(True, False)
+
+    def tell(step, carry):
+        target = lax.rem(sp + step, n_sp)
+        read_copy(target, sp).start()
+        return carry
+
+    lax.fori_loop(1, n_sp, tell, 0)
+    read_land[sp] = read_buf[...]
+
+    def freed(t, carry):
+        for way in range(2):
+            direct(t, way).wait_send()
+            passed(t, way).wait_send()
+        return carry
+
+    lax.fori_loop(0, prompts, freed, 0)
+
+    def sent(t, carry):
+        rev = last - t
+
+        @pl.when(sp + rev <= last)
+        def _():
+            up_copy(t, 0).wait_send()
+
+            @pl.when(core == 0)
+            def _():
+                up_copy(t, 1).wait_send()
+
+        @pl.when(sp >= rev)
+        def _():
+            for part in range(3):
+                down_copy(t, part).wait_send()
+
+            @pl.when(core == 1)
+            def _():
+                down_copy(t, 3).wait_send()
+
+        return carry
+
+    lax.fori_loop(0, last, sent, 0)
+
+    def told(step, carry):
+        source = lax.rem(sp + step, n_sp)
+        read_copy(source, source).wait_recv()
+        read_copy(source, sp).wait_send()
+        return carry
+
+    lax.fori_loop(1, n_sp, told, 0)
+    for h in range(nh):
+        read_out[:, h * DV : (h + 1) * DV] = read_land[:, h].astype(BF)
+
+
+def close_by(n_sp, n_tp, prompts, seg, rows, nh):
+    even = n_sp >= 2 and n_sp & (n_sp - 1) == 0 and seg & (seg - 1) == 0
+    return even and n_tp == 4 and prompts == n_sp and rows == DK and nh <= 8 and seg >= 8
+
+
 def shards(
     n_sp,
     n_tp,
@@ -527,6 +1077,64 @@
     smem = pl.BlockSpec(memory_space=pltpu.SMEM)
     hbm = pl.BlockSpec(memory_space=pl.ANY)
     dma = pltpu.SemaphoreType.DMA
+    if close_by(n_sp, n_tp, prompts, seg, rows, nh):
+        hops = n_sp - 1
+        return pl.pallas_call(
+            functools.partial(near, n_sp, n_tp, nh),
+            out_shape=(
+                jax.ShapeDtypeStruct((rows, nh * DV), BF),
+                jax.ShapeDtypeStruct((prompts, nh * DV), BF),
+            ),
+            in_specs=[hbm, hbm, hbm, vmem, smem, smem, vmem, vmem, vmem],
+            out_specs=(vmem, vmem),
+            scratch_shapes=[
+                pltpu.VMEM((n_tp, prompts, seg, depth), BF),
+                pltpu.VMEM((whole_depth, nh * (DK + DV)), BF),
+                pltpu.VMEM((whole_depth // 128, 2 * heads + 8, 128), F32),
+                pltpu.VMEM((16, whole_depth), BF),
+                pltpu.VMEM((2, 8, seg), F32),
+                pltpu.VMEM((seg, seg), jnp.int32),
+                pltpu.VMEM((seg, seg), BF),
+                pltpu.VMEM((2, seg, nh * (DK + DV)), F32),
+                pltpu.VMEM((2, 16, seg), F32),
+                pltpu.VMEM((prompts, nh, DK, DK), BF),
+                pltpu.VMEM((prompts, nh, DK, DV), F32),
+                pltpu.VMEM((prompts, 8, DV), F32),
+                pltpu.VMEM((hops, 2, nh, DK, DV), BF),
+                pltpu.VMEM((hops, 2, nh, DK, DV), BF),
+                pltpu.VMEM((hops, nh, DK, DK), BF),
+                pltpu.VMEM((hops, nh, DK, DK), BF),
+                pltpu.VMEM((hops, 2, nh, DK, DV), BF),
+                pltpu.VMEM((hops, 2, nh, DK, DV), BF),
+                pltpu.VMEM((hops, 8, DV), F32),
+                pltpu.VMEM((hops, 8, DV), F32),
+                pltpu.VMEM((nh, 8, DK), F32),
+                pltpu.VMEM((8, DV), F32),
+                pltpu.VMEM((prompts, 8, DV), F32),
+                dma((3,)),
+                dma((4, prompts)),
+                dma((4, prompts)),
+                dma((2, hops)),
+                dma((2, hops)),
+                dma((4, hops)),
+                dma((4, hops)),
+                dma((n_sp,)),
+                dma((n_sp,)),
+            ],
+            compiler_params=pltpu.CompilerParams(
+                collective_id=0, has_side_effects=True, vmem_limit_bytes=56 * 1024 * 1024
+            ),
+        )(
+            layer_input,
+            w_key,
+            w_value,
+            gates,
+            decay_rate,
+            beta_bias,
+            log_decay_extra,
+            new_query,
+            read_gain.reshape(1, DV),
+        )
     return pl.pallas_call(
         functools.partial(kernel, n_sp, n_tp, nh, rows),
         out_shape=(

time: 72.1 us -> 58.1 us (0.81)
  Pallas kernels: 68.4 us -> 54.4 us
    pallas_call x1, Pallas kernels: 68.4 us -> 54.4 us  [shards(): pl.pallas_call(functools.partial(near, n_sp, n_tp, nh), out_shape=(jax.Sh...]
where the time goes in v1:
time: 58.1 us; the launch traced here: 57.9 us
  Pallas kernels  54.4 us (94%)
  local copies, waits for them, and re-layouts  2.86 us (5%)
  between operations  0.64 us (1%)
    pallas_call x1, Pallas kernels, shards(): pl.pallas_call(functools.partial(near, n_sp, n_tp, nh), out_shape=(jax.Sh...  54.4 us
    unnamed x2, local copies, waits for them, and re-layouts  2.86 us

profile of v1, /device:TPU:0, one launch (start us, length us, event | category | flops | bytes accessed | tf_op | source)
XLA Modules:
  0.0 57.9 jit_solution(2571966370188253611)
XLA Ops:
  0.6 54.4 %shard_map.104 = (bf16[128,512]{1,0:T(8,128)(2,1)}, bf16[8,512]{1,0:T(8,128)(2,1)}) custom-call(bf16[8,128,512]{2,1,0:T(8,128)(2,1)} %x_hbm.1, bf16[2048,512]{1,0:T(8,128)(2,1)} %wk_hbm.1, bf16[2048,512]{1,0:T(8,128)(2,1)} %wv_hbm.1, bf16[32,2048]{1,0:T(8,128)(2,1)} %bitcast.4, f32[4]{0:T(128)} %rate_ref.1, f32[4]{0:T(128)} %bias_ref.1, ...), custom_call_target="tpu_custom_call" | custom-call | tf_op jit(solution)/shard_map/pallas_call | solution.py:1082
  55.1 1.6 %copy.13 = bf16[128,512]{1,0:T(8,128)(2,1)} copy(bf16[128,512]{1,0:T(8,128)(2,1)} %get-tuple-element.4) | data formatting | bytes 262144
  56.6 1.3 %copy.14 = bf16[8,512]{1,0:T(8,128)(2,1)} copy(bf16[8,512]{1,0:T(8,128)(2,1)} %get-tuple-element.5) | data formatting | bytes 16384

commit v2 on v1

--- a/solution.py
+++ b/solution.py
@@ -510,14 +510,20 @@
     x_hbm,
     wk_hbm,
     wv_hbm,
+    gates_hbm,
+    rate_hbm,
+    bias_hbm,
+    extra_hbm,
+    query_hbm,
+    gain_hbm,
+    state_out,
+    read_out,
     gates_ref,
     rate_ref,
     bias_ref,
     extra_ref,
     query_ref,
     gain_ref,
-    state_out,
-    read_out,
     gath,
     w,
     gall,
@@ -532,16 +538,13 @@
     decs,
     up_out,
     up_in,
-    map_out,
-    map_in,
-    add_out,
-    add_in,
-    dec_out,
-    dec_in,
+    down_out,
+    down_in,
     query,
     read_buf,
     read_land,
     local_sem,
+    x_sem,
     gsend,
     grecv,
     usend,
@@ -559,90 +562,69 @@
     sp = lax.axis_index("sp")
     tp = lax.axis_index("tp")
     core = lax.rem(sp, 2)
-
-    x_copy = pltpu.make_async_copy(x_hbm, gath.at[tp], local_sem.at[0])
-    x_copy.start()
-    wk_copy = pltpu.make_async_copy(wk_hbm, w.at[:, pl.ds(0, width)], local_sem.at[1])
-    wv_copy = pltpu.make_async_copy(wv_hbm, w.at[:, pl.ds(width, nh * DV)], local_sem.at[2])
-    wk_copy.start()
-    wv_copy.start()
+    chip = sp // 2
+    chips = n_sp // 2
+    map_at = 4 * pad
+    add_at = map_at + nh * DK
+    low_at = add_at + nh * DK
+
+    def prompt_at(t):
+        rev = chips - 1 - t // 2
+        owner = 0
+        k = 1
+        while k < chips:
+            owner = owner + k * lax.rem(chip // k + rev // k, 2)
+            k *= 2
+        flip = (2 * (owner - chip) + 1 - core + n_sp - 1) // n_sp
+        return 2 * owner + lax.rem(flip + lax.rem(t, 2), 2)
+
+    def x_copy(t):
+        p = prompt_at(t)
+        return pltpu.make_async_copy(
+            x_hbm.at[p], gath.at[tp, p], x_sem.at[min(t, early)]
+        )
+
+    early = min(2, prompts)
+    for t in range(prompts):
+        x_copy(t).start()
 
     barrier = pltpu.get_barrier_semaphore()
     xn = tp + 1 - 2 * lax.rem(tp, 2)
     yn = tp + 2 - 4 * (tp // 2)
     far = n_tp - 1 - tp
 
-    pl.semaphore_signal(barrier, inc=1, device_id={"tp": xn})
-    pl.semaphore_signal(barrier, inc=1, device_id={"tp": yn})
-
     def greet_sp(step, carry):
         pl.semaphore_signal(barrier, inc=1, device_id={"sp": lax.rem(sp + step, n_sp)})
         return carry
 
     lax.fori_loop(1, n_sp, greet_sp, 0)
-
-    r_id = lax.broadcasted_iota(jnp.int32, (seg, seg), 0)
-    c_id = lax.broadcasted_iota(jnp.int32, (seg, seg), 1)
-    lev = jnp.zeros((seg, seg), jnp.int32)
-    k = 1
-    while (1 << k) < seg:
-        lev = jnp.where((r_id >> k) != (c_id >> k), k, lev)
-        k += 1
-    levels = k
-    level[...] = jnp.where(r_id > c_id, lev, -1)
-    upper[...] = jnp.where(r_id <= c_id, 1.0, 0.0).astype(BF)
-    groups = [(k, min(k + 3, levels)) for k in range(1, levels, 3)]
-
-    row_id = lax.broadcasted_iota(jnp.int32, (pad, seg), 0)
-    rate = jnp.zeros((pad, seg), F32)
-    bias = jnp.zeros((pad, seg), F32)
-    for h in range(nh):
-        rate = jnp.where(row_id == h, rate_ref[h], rate)
-        bias = jnp.where(row_id == h, bias_ref[h], bias)
-    fixed[0] = rate
-    fixed[1] = bias
-    for at in range(n_tp * depth // 128):
-        part = gates_ref[:, at * 128 : (at + 1) * 128].astype(F32)
-        gall[at, pl.ds(0, heads)] = part[:heads]
-        gall[at, pl.ds(heads, heads)] = part[heads:]
-        gall[at, pl.ds(2 * heads, pad)] = jnp.zeros((pad, 128), F32)
-        picked = [gall[at, pl.ds(tp * nh + k * heads, pad)] for k in range(2)]
-        gsel[:, at * 128 : (at + 1) * 128] = jnp.concatenate(picked, axis=0).astype(BF)
-    every = query_ref[...].astype(F32)
-    mine = lax.broadcasted_iota(jnp.int32, every.shape, 0) == sp
-    asked = jnp.sum(jnp.where(mine, every, 0.0), axis=0, keepdims=True)
-    for h in range(nh):
-        query[h] = jnp.broadcast_to(asked[:, h * DK : (h + 1) * DK], (pad, DK))
-    read_buf[...] = jnp.zeros_like(read_buf)
-
-    @pl.when(core == 0)
-    def _():
-        up_in[:, 1] = jnp.zeros((n_sp - 1, nh, DK, DV), BF)
-
-    @pl.when(core == 1)
-    def _():
-        add_in[:, 1] = jnp.zeros((n_sp - 1, nh, DK, DV), BF)
-
+    pl.semaphore_signal(barrier, inc=1, device_id={"tp": xn})
+    pl.semaphore_signal(barrier, inc=1, device_id={"tp": yn})
+    loads = [
+        pltpu.make_async_copy(source, target, local_sem.at[k])
+        for k, (source, target) in enumerate(
+            (
+                (gates_hbm, gates_ref),
+                (rate_hbm, rate_ref),
+                (bias_hbm, bias_ref),
+                (extra_hbm, extra_ref),
+                (query_hbm, query_ref),
+                (gain_hbm, gain_ref),
+                (wk_hbm, w.at[:, pl.ds(0, width)]),
+                (wv_hbm, w.at[:, pl.ds(width, nh * DV)]),
+            )
+        )
+    ]
     pl.semaphore_wait(barrier, 2 + n_sp - 1)
-    x_copy.wait()
 
     half = seg // 2
-
-    def prompt_at(t):
-        rev = last - t
-        p = 0
-        k = 1
-        while k < n_sp:
-            p = p + k * lax.rem(sp // k + rev // k, 2)
-            k *= 2
-        return p
 
     def direct(t, way):
         p = prompt_at(t)
         return pltpu.make_async_remote_copy(
             src_ref=gath.at[tp, p],
             dst_ref=gath.at[tp, p],
-            send_sem=gsend.at[way, t],
+            send_sem=gsend.at[0],
             recv_sem=grecv.at[way, t],
             device_id={"tp": xn if way == 0 else yn},
         )
@@ -654,8 +636,8 @@
         return pltpu.make_async_remote_copy(
             src_ref=gath.at[source, p, part],
             dst_ref=gath.at[source, p, part],
-            send_sem=gsend.at[2 + way, t],
-            recv_sem=grecv.at[2 + way, t],
+            send_sem=gsend.at[0],
+            recv_sem=grecv.at[2, t],
             device_id={"tp": yn if way == 0 else xn},
         )
 
@@ -669,42 +651,55 @@
         direct(t, 1).wait_recv()
         passed(t, 1).start()
 
-    def up_copy(t, part):
+    def gathered(t):
+        block = gath.at[far, prompt_at(t)]
+        pltpu.make_async_remote_copy(
+            src_ref=block,
+            dst_ref=block,
+            send_sem=gsend.at[0],
+            recv_sem=grecv.at[2, t],
+            device_id={"tp": xn},
+        ).wait_recv()
+
+    def up_copy(t, full):
         return pltpu.make_async_remote_copy(
-            src_ref=up_out.at[t, part],
-            dst_ref=up_in.at[t, part],
-            send_sem=usend.at[part, t],
-            recv_sem=urecv.at[part, t],
+            src_ref=up_out.at[t] if full else up_out.at[t, 0],
+            dst_ref=up_in.at[t] if full else up_in.at[t, 0],
+            send_sem=usend.at[lax.rem(t, 2)],
+            recv_sem=urecv.at[t],
             device_id={"sp": sp + 1},
         )
 
-    def down_copy(t, part):
-        pairs = (
-            (map_out.at[t], map_in.at[t]),
-            (add_out.at[t, 0], add_in.at[t, 0]),
-            (dec_out.at[t], dec_in.at[t]),
-            (add_out.at[t, 1], add_in.at[t, 1]),
-        )
+    def down_copy(t, full):
+        part = pl.ds(0, down_out.shape[1] if full else low_at)
         return pltpu.make_async_remote_copy(
-            src_ref=pairs[part][0],
-            dst_ref=pairs[part][1],
-            send_sem=dsend.at[part, t],
-            recv_sem=drecv.at[part, t],
+            src_ref=down_out.at[t, part],
+            dst_ref=down_in.at[t, part],
+            send_sem=dsend.at[lax.rem(t, 2)],
+            recv_sem=drecv.at[t],
             device_id={"sp": sp - 1},
         )
+
+    def on_core(which, act):
+        pl.when(core == which)(lambda: act(True))
+        pl.when(core != which)(lambda: act(False))
 
     def read_copy(target, source):
         return pltpu.make_async_remote_copy(
             src_ref=read_buf,
             dst_ref=read_land.at[source],
-            send_sem=rsend.at[target],
-            recv_sem=rrecv.at[source],
+            send_sem=rsend.at[0],
+            recv_sem=rrecv.at[0],
             device_id={"sp": target},
         )
 
     def band(source):
         return pl.ds(pl.multiple_of(source * depth, depth), depth)
 
+    levels = 1
+    while (1 << levels) < seg:
+        levels += 1
+    groups = [(k, min(k + 3, levels)) for k in range(1, levels, 3)]
     tile = DK + DV
     near_by = (tp, xn, yn)
 
@@ -848,48 +843,48 @@
             up_out[t, 0, h] = top
             up_out[t, 1, h] = (state - top.astype(F32)).astype(BF)
 
+    def later(at):
+        part = down_in[at, pl.ds(0, map_at)].astype(F32)
+        return part[:pad] + part[pad : 2 * pad] + part[2 * pad : 3 * pad]
+
+    def rows(first, h):
+        return pl.ds(first + h * DK, DK)
+
+    def total(at, h):
+        top = down_in[at, rows(add_at, h)].astype(F32)
+        return top + down_in[at, rows(low_at, h)].astype(F32)
+
     def go_down(t, p, fresh):
+        own = decs[p]
+        dec = None if fresh else later(t - 1)
         for h in range(nh):
+            add = adds[p, h]
             if fresh:
-                total = adds[p, h]
-                map_out[t, h] = maps[p, h]
+                down_out[t, rows(map_at, h)] = maps[p, h]
             else:
-                own = decs[p, pl.ds(h, 1)]
-                later = dec_in[t - 1, pl.ds(h, 1)]
-                late = map_in[t - 1, h]
+                late = down_in[t - 1, rows(map_at, h)]
                 early = maps[p, h]
-                add = adds[p, h]
                 turn = dot(late, jnp.concatenate([early, add.astype(BF)], axis=1))
-                total = (
-                    later * add
-                    + add_in[t - 1, 0, h].astype(F32)
-                    + add_in[t - 1, 1, h].astype(F32)
-                    - turn[:, DK:]
-                )
-                map_out[t, h] = (
-                    later * early.astype(F32) + own * late.astype(F32) - turn[:, :DK]
-                ).astype(BF)
-            top = total.astype(BF)
-            add_out[t, 0, h] = top
-            add_out[t, 1, h] = (total - top.astype(F32)).astype(BF)
-        dec_out[t] = decs[p] if fresh else decs[p] * dec_in[t - 1]
+                add = dec[h : h + 1] * add + total(t - 1, h) - turn[:, DK:]
+                both = dec[h : h + 1] * early.astype(F32) + own[h : h + 1] * late.astype(F32)
+                down_out[t, rows(map_at, h)] = (both - turn[:, :DK]).astype(BF)
+            top = add.astype(BF)
+            down_out[t, rows(add_at, h)] = top
+            down_out[t, rows(low_at, h)] = (add - top.astype(F32)).astype(BF)
+        dec = own if fresh else own * dec
+        high = dec.astype(BF).astype(F32)
+        rest = dec - high
+        mid = rest.astype(BF).astype(F32)
+        split = jnp.concatenate([high, mid, rest - mid, jnp.zeros_like(high)], axis=0)
+        down_out[t, pl.ds(0, map_at)] = split.astype(BF)
 
     def wait_up(t):
-        up_copy(t, 0).wait_recv()
-
-        @pl.when(core == 1)
-        def _():
-            up_copy(t, 1).wait_recv()
+        on_core(1, lambda full: up_copy(t, full).wait_recv())
 
     def wait_down(t):
-        for part in range(3):
-            down_copy(t, part).wait_recv()
-
-        @pl.when(core == 0)
-        def _():
-            down_copy(t, 3).wait_recv()
-
-    def chain(t):
+        on_core(0, lambda full: down_copy(t, full).wait_recv())
+
+    def chain_up(t):
         rev = last - t
 
         @pl.when(sp + rev <= last)
@@ -903,11 +898,14 @@
                 wait_up(t - 1)
                 go_up(t, sp + rev, False)
 
-            up_copy(t, 0).start()
-
-            @pl.when(core == 0)
+            @pl.when(sp + rev + 2 <= last)
             def _():
-                up_copy(t, 1).start()
+                on_core(0, lambda full: up_copy(t - 2, full).wait_send())
+
+            on_core(0, lambda full: up_copy(t, full).start())
+
+    def chain_down(t):
+        rev = last - t
 
         @pl.when(sp >= rev)
         def _():
@@ -920,23 +918,30 @@
                 wait_down(t - 1)
                 go_down(t, sp - rev, False)
 
-            for part in range(3):
-                down_copy(t, part).start()
-
-            @pl.when(core == 1)
+            @pl.when(sp >= rev + 2)
             def _():
-                down_copy(t, 3).start()
+                on_core(1, lambda full: down_copy(t - 2, full).wait_send())
+
+            on_core(1, lambda full: down_copy(t, full).start())
+
+    def before(t):
+        pl.when(core == 0)(lambda: chain_down(t))
+        pl.when(core == 1)(lambda: chain_up(t))
+
+    def after(t):
+        pl.when(core == 0)(lambda: chain_up(t))
+        pl.when(core == 1)(lambda: chain_down(t))
 
     def close(below, above):
         at = last - 1
+        dec = later(at) if above else None
         for h in range(nh):
             state = moved(at, sp, h) if below else adds[sp, h]
             if above:
                 state = (
-                    dec_in[at, pl.ds(h, 1)] * state
-                    + add_in[at, 0, h].astype(F32)
-                    + add_in[at, 1, h].astype(F32)
-                    - dot(map_in[at, h], state.astype(BF))
+                    dec[h : h + 1] * state
+                    + total(at, h)
+                    - dot(down_in[at, rows(map_at, h)], state.astype(BF))
                 )
             cached = state.astype(BF)
             state_out[:, h * DV : (h + 1) * DV] = cached
@@ -948,14 +953,65 @@
             )
             read_buf[pl.ds(h, 1)] = norm[:1]
 
-    early = min(2, prompts)
     for t in range(early):
+        x_copy(t).wait()
         start_direct(t)
+    for load in loads:
+        load.start()
+    if early < prompts:
+        others = pl.ds(0, prompts - early)
+        pltpu.make_async_copy(
+            x_hbm.at[others], gath.at[tp, others], x_sem.at[early]
+        ).wait()
+    for load in loads[:6]:
+        load.wait()
+
+    r_id = lax.broadcasted_iota(jnp.int32, (seg, seg), 0)
+    c_id = lax.broadcasted_iota(jnp.int32, (seg, seg), 1)
+    lev = jnp.zeros((seg, seg), jnp.int32)
+    k = 1
+    while (1 << k) < seg:
+        lev = jnp.where((r_id >> k) != (c_id >> k), k, lev)
+        k += 1
+    level[...] = jnp.where(r_id > c_id, lev, -1)
+    upper[...] = jnp.where(r_id <= c_id, 1.0, 0.0).astype(BF)
+
+    row_id = lax.broadcasted_iota(jnp.int32, (pad, seg), 0)
+    rate = jnp.zeros((pad, seg), F32)
+    bias = jnp.zeros((pad, seg), F32)
+    for h in range(nh):
+        rate = jnp.where(row_id == h, rate_ref[h], rate)
+        bias = jnp.where(row_id == h, bias_ref[h], bias)
+    fixed[0] = rate
+    fixed[1] = bias
+    for at in range(n_tp * depth // 128):
+        part = gates_ref[:, at * 128 : (at + 1) * 128].astype(F32)
+        gall[at, pl.ds(0, heads)] = part[:heads]
+        gall[at, pl.ds(heads, heads)] = part[heads:]
+        gall[at, pl.ds(2 * heads, pad)] = jnp.zeros((pad, 128), F32)
+        picked = [gall[at, pl.ds(tp * nh + k * heads, pad)] for k in range(2)]
+        gsel[:, at * 128 : (at + 1) * 128] = jnp.concatenate(picked, axis=0).astype(BF)
+    every = query_ref[...].astype(F32)
+    mine = lax.broadcasted_iota(jnp.int32, every.shape, 0) == sp
+    asked = jnp.sum(jnp.where(mine, every, 0.0), axis=0, keepdims=True)
+    for h in range(nh):
+        query[h] = jnp.broadcast_to(asked[:, h * DK : (h + 1) * DK], (pad, DK))
+    read_buf[...] = jnp.zeros_like(read_buf)
+
+    @pl.when(core == 0)
+    def _():
+        up_in[:, 1] = jnp.zeros((n_sp - 1, nh, DK, DV), BF)
+
+    @pl.when(core == 1)
+    def _():
+        down_in[:, pl.ds(low_at, nh * DK)] = jnp.zeros((n_sp - 1, nh * DK, DV), BF)
+
+
     pass_on(0)
     if early < prompts:
         start_direct(early)
-    wk_copy.wait()
-    wv_copy.wait()
+    for load in loads[6:]:
+        load.wait()
     for go in ahead(0):
         go()
 
@@ -966,15 +1022,14 @@
         def _():
             start_direct(t + 1 + early)
 
-        passed(t, 0).wait_recv()
-        passed(t, 1).wait_recv()
+        gathered(t)
+        before(t)
         work(t, ahead(t + 1))
-        chain(t)
+        after(t)
         return carry
 
     lax.fori_loop(0, last, body, 0)
-    passed(last, 0).wait_recv()
-    passed(last, 1).wait_recv()
+    gathered(last)
     work(last, [])
 
     @pl.when(sp > 0)
@@ -1005,45 +1060,35 @@
     lax.fori_loop(1, n_sp, tell, 0)
     read_land[sp] = read_buf[...]
 
-    def freed(t, carry):
-        for way in range(2):
-            direct(t, way).wait_send()
-            passed(t, way).wait_send()
-        return carry
-
-    lax.fori_loop(0, prompts, freed, 0)
-
-    def sent(t, carry):
-        rev = last - t
-
-        @pl.when(sp + rev <= last)
+    block = gath.at[pl.ds(0, n_tp - 1)]
+    pltpu.make_async_remote_copy(
+        src_ref=block,
+        dst_ref=block,
+        send_sem=gsend.at[0],
+        recv_sem=grecv.at[2, 0],
+        device_id={"tp": xn},
+    ).wait_send()
+
+    for back in range(1, min(last, 2) + 1):
+
+        @pl.when(sp + back <= last)
         def _():
-            up_copy(t, 0).wait_send()
-
-            @pl.when(core == 0)
-            def _():
-                up_copy(t, 1).wait_send()
-
-        @pl.when(sp >= rev)
+            on_core(0, lambda full: up_copy(last - back, full).wait_send())
+
+        @pl.when(sp >= back)
         def _():
-            for part in range(3):
-                down_copy(t, part).wait_send()
-
-            @pl.when(core == 1)
-            def _():
-                down_copy(t, 3).wait_send()
-
-        return carry
-
-    lax.fori_loop(0, last, sent, 0)
-
-    def told(step, carry):
-        source = lax.rem(sp + step, n_sp)
-        read_copy(source, source).wait_recv()
-        read_copy(source, sp).wait_send()
-        return carry
-
-    lax.fori_loop(1, n_sp, told, 0)
+            on_core(1, lambda full: down_copy(last - back, full).wait_send())
+
+    others = read_land.at[pl.ds(0, last)]
+    reads = pltpu.make_async_remote_copy(
+        src_ref=others,
+        dst_ref=others,
+        send_sem=rsend.at[0],
+        recv_sem=rrecv.at[0],
+        device_id={"sp": lax.rem(sp + 1, n_sp)},
+    )
+    reads.wait_send()
+    reads.wait_recv()
     for h in range(nh):
         read_out[:, h * DV : (h + 1) * DV] = read_land[:, h].astype(BF)
 
@@ -1082,12 +1127,18 @@
         return pl.pallas_call(
             functools.partial(near, n_sp, n_tp, nh),
             out_shape=(
-                jax.ShapeDtypeStruct((rows, nh * DV), BF),
-                jax.ShapeDtypeStruct((prompts, nh * DV), BF),
+                pltpu.VMEM((rows, nh * DV), BF),
+                pltpu.VMEM((prompts, nh * DV), BF),
             ),
-            in_specs=[hbm, hbm, hbm, vmem, smem, smem, vmem, vmem, vmem],
+            in_specs=[hbm] * 9,
             out_specs=(vmem, vmem),
             scratch_shapes=[
+                pltpu.VMEM((2 * heads, whole_depth), BF),
+                pltpu.SMEM((nh,), F32),
+                pltpu.SMEM((nh,), F32),
+                pltpu.VMEM((prompts, nh, seg), F32),
+                pltpu.VMEM((prompts, nh * DK), BF),
+                pltpu.VMEM((1, DV), F32),
                 pltpu.VMEM((n_tp, prompts, seg, depth), BF),
                 pltpu.VMEM((whole_depth, nh * (DK + DV)), BF),
                 pltpu.VMEM((whole_depth // 128, 2 * heads + 8, 128), F32),
@@ -1102,24 +1153,21 @@
                 pltpu.VMEM((prompts, 8, DV), F32),
                 pltpu.VMEM((hops, 2, nh, DK, DV), BF),
                 pltpu.VMEM((hops, 2, nh, DK, DV), BF),
-                pltpu.VMEM((hops, nh, DK, DK), BF),
-                pltpu.VMEM((hops, nh, DK, DK), BF),
-                pltpu.VMEM((hops, 2, nh, DK, DV), BF),
-                pltpu.VMEM((hops, 2, nh, DK, DV), BF),
-                pltpu.VMEM((hops, 8, DV), F32),
-                pltpu.VMEM((hops, 8, DV), F32),
+                pltpu.VMEM((hops, 32 + 3 * nh * DK, DV), BF),
+                pltpu.VMEM((hops, 32 + 3 * nh * DK, DV), BF),
                 pltpu.VMEM((nh, 8, DK), F32),
                 pltpu.VMEM((8, DV), F32),
                 pltpu.VMEM((prompts, 8, DV), F32),
-                dma((3,)),
-                dma((4, prompts)),
-                dma((4, prompts)),
-                dma((2, hops)),
-                dma((2, hops)),
-                dma((4, hops)),
-                dma((4, hops)),
-                dma((n_sp,)),
-                dma((n_sp,)),
+                dma((8,)),
+                dma((min(2, prompts) + 1,)),
+                dma((1,)),
+                dma((3, prompts)),
+                dma((2,)),
+                dma((hops,)),
+                dma((2,)),
+                dma((hops,)),
+                dma((1,)),
+                dma((1,)),
             ],
             compiler_params=pltpu.CompilerParams(
                 collective_id=0, has_side_effects=True, vmem_limit_bytes=56 * 1024 * 1024

time: 58.1 us -> 52.2 us (0.90)
  Pallas kernels: 54.4 us -> 50.2 us
  local copies, waits for them, and re-layouts: 2.86 us -> 1.26 us
    pallas_call x1, Pallas kernels: 54.4 us -> 50.2 us  [shards(): pl.pallas_call(functools.partial(near, n_sp, n_tp, nh), out_shape=(pltpu....]
    unnamed x2, local copies, waits for them, and re-layouts: 2.86 us -> 1.26 us
where the time goes in v2:
time: 52.2 us; the launch traced here: 52.1 us
  Pallas kernels  50.2 us (96%)
  local copies, waits for them, and re-layouts  1.26 us (2%)
  between operations  0.64 us (1%)
    pallas_call x1, Pallas kernels, shards(): pl.pallas_call(functools.partial(near, n_sp, n_tp, nh), out_shape=(pltpu....  50.2 us
    unnamed x2, local copies, waits for them, and re-layouts  1.26 us

profile of v2, /device:TPU:0, one launch (start us, length us, event | category | flops | bytes accessed | tf_op | source)
XLA Modules:
  0.0 52.1 jit_solution(18192305389271480784)
XLA Ops:
  0.6 50.2 %shard_map.104 = (bf16[128,512]{1,0:T(8,128)(2,1)S(1)}, bf16[8,512]{1,0:T(8,128)(2,1)S(1)}) custom-call(bf16[8,128,512]{2,1,0:T(8,128)(2,1)} %x_hbm.1, bf16[2048,512]{1,0:T(8,128)(2,1)} %wk_hbm.1, bf16[2048,512]{1,0:T(8,128)(2,1)} %wv_hbm.1, bf16[32,2048]{1,0:T(8,128)(2,1)} %bitcast.4, f32[4]{0:T(128)} %rate_hbm.1, f32[4]{0:T(128)} %bias_hbm.1, ...), custom_call_target="tpu_custom_call" | custom-call | tf_op jit(solution)/shard_map/pallas_call | solution.py:1127
  50.8 0.7 %copy.13 = bf16[128,512]{1,0:T(8,128)(2,1)} copy(bf16[128,512]{1,0:T(8,128)(2,1)S(1)} %get-tuple-element.2) | data formatting | bytes 262144
  51.5 0.6 %copy.14 = bf16[8,512]{1,0:T(8,128)(2,1)} copy(bf16[8,512]{1,0:T(8,128)(2,1)S(1)} %get-tuple-element.3) | data formatting | bytes 16384

commit v3 on v2

--- a/solution.py
+++ b/solution.py
@@ -593,11 +593,14 @@
     yn = tp + 2 - 4 * (tp // 2)
     far = n_tp - 1 - tp
 
-    def greet_sp(step, carry):
-        pl.semaphore_signal(barrier, inc=1, device_id={"sp": lax.rem(sp + step, n_sp)})
-        return carry
-
-    lax.fori_loop(1, n_sp, greet_sp, 0)
+    @pl.when(sp > 0)
+    def _():
+        pl.semaphore_signal(barrier, inc=1, device_id={"sp": sp - 1})
+
+    @pl.when(sp < last)
+    def _():
+        pl.semaphore_signal(barrier, inc=1, device_id={"sp": sp + 1})
+
     pl.semaphore_signal(barrier, inc=1, device_id={"tp": xn})
     pl.semaphore_signal(barrier, inc=1, device_id={"tp": yn})
     loads = [
@@ -615,47 +618,49 @@
             )
         )
     ]
-    pl.semaphore_wait(barrier, 2 + n_sp - 1)
-
-    half = seg // 2
-
-    def direct(t, way):
+    beside = (sp + last - 1) // last + (2 * last - sp - 1) // last
+    pl.semaphore_wait(barrier, 2 + beside)
+
+    half = depth // 2
+
+    def part(at):
+        return pl.ds(at * half, half)
+
+    def direct(t, way, first):
         p = prompt_at(t)
+        block = gath.at[tp, p, :, part(way if first else 1 - way)]
         return pltpu.make_async_remote_copy(
-            src_ref=gath.at[tp, p],
-            dst_ref=gath.at[tp, p],
+            src_ref=block,
+            dst_ref=block,
             send_sem=gsend.at[0],
-            recv_sem=grecv.at[way, t],
+            recv_sem=grecv.at[way, t] if first else grecv.at[2, t],
             device_id={"tp": xn if way == 0 else yn},
         )
 
     def passed(t, way):
-        p = prompt_at(t)
-        source = xn if way == 0 else yn
-        part = pl.ds(way * half, half)
+        block = gath.at[xn if way == 0 else yn, prompt_at(t), :, part(way)]
         return pltpu.make_async_remote_copy(
-            src_ref=gath.at[source, p, part],
-            dst_ref=gath.at[source, p, part],
+            src_ref=block,
+            dst_ref=block,
             send_sem=gsend.at[0],
             recv_sem=grecv.at[2, t],
             device_id={"tp": yn if way == 0 else xn},
         )
 
-    def start_direct(t):
-        direct(t, 0).start()
-        direct(t, 1).start()
+    def start_direct(t, first):
+        for way in range(2):
+            direct(t, way, first).start()
 
     def pass_on(t):
-        direct(t, 0).wait_recv()
-        passed(t, 0).start()
-        direct(t, 1).wait_recv()
-        passed(t, 1).start()
+        for way in range(2):
+            direct(t, way, True).wait_recv()
+            passed(t, way).start()
 
     def gathered(t):
-        block = gath.at[far, prompt_at(t)]
+        blocks = gath.at[pl.ds(0, 2), prompt_at(t)]
         pltpu.make_async_remote_copy(
-            src_ref=block,
-            dst_ref=block,
+            src_ref=blocks,
+            dst_ref=blocks,
             send_sem=gsend.at[0],
             recv_sem=grecv.at[2, t],
             device_id={"tp": xn},
@@ -671,10 +676,10 @@
         )
 
     def down_copy(t, full):
-        part = pl.ds(0, down_out.shape[1] if full else low_at)
+        span = pl.ds(0, down_out.shape[1] if full else low_at)
         return pltpu.make_async_remote_copy(
-            src_ref=down_out.at[t, part],
-            dst_ref=down_in.at[t, part],
+            src_ref=down_out.at[t, span],
+            dst_ref=down_in.at[t, span],
             send_sem=dsend.at[lax.rem(t, 2)],
             recv_sem=drecv.at[t],
             device_id={"sp": sp - 1},
@@ -693,30 +698,39 @@
             device_id={"sp": target},
         )
 
-    def band(source):
-        return pl.ds(pl.multiple_of(source * depth, depth), depth)
+    soon = ((tp, 0), (tp, 1), (xn, 0), (yn, 1))
+    late = ((far, 0), (far, 1), (xn, 1), (yn, 0))
+
+    def feature(at):
+        return pl.ds(pl.multiple_of(at[0] * depth + at[1] * half, half), half)
+
+    def features(p, which):
+        return jnp.concatenate([gath[s, p, :, part(k)] for s, k in which], axis=1)
+
+    def gate_rows(which):
+        return jnp.concatenate([gsel[:, feature(at)] for at in which], axis=1)
+
+    def weights(which, cols):
+        return jnp.concatenate([w[feature(at), cols] for at in which], axis=0)
 
     levels = 1
     while (1 << levels) < seg:
         levels += 1
     groups = [(k, min(k + 3, levels)) for k in range(1, levels, 3)]
     tile = DK + DV
-    near_by = (tp, xn, yn)
 
     def ahead(t):
         p = prompt_at(t)
         slot = lax.rem(t, 2)
-        x = jnp.concatenate([gath[s, p] for s in near_by], axis=1)
+        x = features(p, soon)
 
         def gate_piece():
-            g = jnp.concatenate([gsel[:, band(s)] for s in near_by], axis=1)
-            gacc[slot] = dot(g, x, ((1,), (1,)))
+            gacc[slot] = dot(gate_rows(soon), x, ((1,), (1,)))
 
         def piece(at):
             def go():
                 cols = pl.ds(at * tile, tile)
-                side = jnp.concatenate([w[band(s), cols] for s in near_by], axis=0)
-                acc[slot, :, cols] = dot(x, side)
+                acc[slot, :, cols] = dot(x, weights(soon, cols))
 
             return go
 
@@ -731,16 +745,17 @@
 
         p = prompt_at(t)
         slot = lax.rem(t, 2)
-        x = gath[far, p]
-        gt = gacc[slot] + dot(gsel[:, band(far)], x, ((1,), (1,)))
-        key_pre = acc[slot, :, :width] + dot(x, w[band(far), :width])
-        value_pre = acc[slot, :, width:] + dot(x, w[band(far), width:])
+        x = features(p, late)
+        gt = gacc[slot] + dot(gate_rows(late), x, ((1,), (1,)))
+        key_pre = acc[slot, :, :width] + dot(x, weights(late, pl.ds(0, width)))
         gd = gt[:pad]
         gb = gt[pad:]
         extra = jnp.concatenate([extra_ref[p], jnp.zeros((pad - nh, seg), F32)], axis=0)
         soft = jnp.maximum(gd, 0.0) + jnp.log1p(jnp.exp(-jnp.abs(gd)))
         log_decay = extra - fixed[0] * soft
-        beta = jax.nn.sigmoid(gb + fixed[1])
+        beta_pre = gb + fixed[1]
+        beta = jax.nn.sigmoid(beta_pre)
+        log_beta = jnp.minimum(beta_pre, 0.0) - jnp.log1p(jnp.exp(-jnp.abs(beta_pre)))
         high = log_decay.astype(BF).astype(F32)
         rest = log_decay - high
         mid = rest.astype(BF).astype(F32)
@@ -750,7 +765,7 @@
         end = run[:, seg - 1 : seg]
         decs[p] = jnp.broadcast_to(jnp.exp(end), (pad, DV))
         cols = jnp.concatenate(
-            [run, beta, beta * jnp.exp(run), jnp.exp(end - run)], axis=0
+            [run + log_beta, beta, beta * jnp.exp(run), jnp.exp(end - run)], axis=0
         ).T
         lev = level[...]
         strict = lev >= 0
@@ -769,13 +784,13 @@
             kb = key.astype(BF)
             keys.append(key)
             grams.append(dot(kb, kb, ((1,), (1,))))
+        value_pre = acc[slot, :, width:] + dot(x, weights(late, pl.ds(width, nh * DV)))
         fill()
         fill()
         lower, inv = [], []
         for h in hs:
             spread = cols[:, h : h + 1] - run[h : h + 1, :]
-            weight = jnp.exp(jnp.where(strict, spread, 0.0))
-            low = jnp.where(strict, grams[h] * weight * cols[:, pad + h : pad + h + 1], 0.0)
+            low = jnp.where(strict, grams[h] * jnp.exp(jnp.where(strict, spread, 0.0)), 0.0)
             lower.append(low)
             inv.append(eye - jnp.where(lev == 0, low, 0.0))
 
@@ -787,11 +802,17 @@
         for first, until in groups[:-1]:
             steps = merge(first, until)
             fill()
-            inv = [f - dot(e, f.astype(BF)) for e, f in zip(steps, inv)]
-            for _ in range(first + 1, until):
-                steps = [dot(e, e).astype(BF) for e in steps]
+            for k in range(first, until - 1):
+                both = [
+                    dot(e, jnp.concatenate([e, f.astype(BF)], axis=1))
+                    for e, f in zip(steps, inv)
+                ]
+                steps = [b[:, :seg].astype(BF) for b in both]
                 fill()
-                inv = [f + dot(e, f.astype(BF)) for e, f in zip(steps, inv)]
+                inv = [f - b[:, seg:] if k == first else f + b[:, seg:] for f, b in zip(inv, both)]
+            one = until - 1 == first
+            moves = [dot(e, f.astype(BF)) for e, f in zip(steps, inv)]
+            inv = [f - m if one else f + m for f, m in zip(inv, moves)]
         sides = []
         for h in hs:
             pre = value_pre[:, h * DV : (h + 1) * DV]
@@ -820,15 +841,17 @@
             fill()
         tall = ((0,), (0,))
         for h in hs:
-            late = keys[h] * cols[:, 3 * pad + h : 3 * pad + h + 1]
-            late_top = late.astype(BF)
-            late_rest = (late - late_top.astype(F32)).astype(BF)
+            faded = keys[h] * cols[:, 3 * pad + h : 3 * pad + h + 1]
+            late_top = faded.astype(BF)
+            late_rest = (faded - late_top.astype(F32)).astype(BF)
             top = sides[h].astype(BF)
             rest = (sides[h][:, :DV] - top[:, :DV].astype(F32)).astype(BF)
-            both = dot(late_top, top, tall)
-            adds[p, h] = (
-                both[:, :DV] + dot(late_top, rest, tall) + dot(late_rest, top[:, :DV], tall)
+            both = dot(
+                jnp.concatenate([late_top, late_rest], axis=0),
+                jnp.concatenate([top, top], axis=0),
+                tall,
             )
+            adds[p, h] = both[:, :DV] + dot(late_top, rest, tall)
             maps[p, h] = both[:, DV:].astype(BF)
 
     def moved(at, p, h):
@@ -844,8 +867,8 @@
             up_out[t, 1, h] = (state - top.astype(F32)).astype(BF)
 
     def later(at):
-        part = down_in[at, pl.ds(0, map_at)].astype(F32)
-        return part[:pad] + part[pad : 2 * pad] + part[2 * pad : 3 * pad]
+        terms = down_in[at, pl.ds(0, map_at)].astype(F32)
+        return terms[:pad] + terms[pad : 2 * pad] + terms[2 * pad : 3 * pad]
 
     def rows(first, h):
         return pl.ds(first + h * DK, DK)
@@ -862,11 +885,11 @@
             if fresh:
                 down_out[t, rows(map_at, h)] = maps[p, h]
             else:
-                late = down_in[t - 1, rows(map_at, h)]
-                early = maps[p, h]
-                turn = dot(late, jnp.concatenate([early, add.astype(BF)], axis=1))
+                above = down_in[t - 1, rows(map_at, h)]
+                own_map = maps[p, h]
+                turn = dot(above, jnp.concatenate([own_map, add.astype(BF)], axis=1))
                 add = dec[h : h + 1] * add + total(t - 1, h) - turn[:, DK:]
-                both = dec[h : h + 1] * early.astype(F32) + own[h : h + 1] * late.astype(F32)
+                both = dec[h : h + 1] * own_map.astype(F32) + own[h : h + 1] * above.astype(F32)
                 down_out[t, rows(map_at, h)] = (both - turn[:, :DK]).astype(BF)
             top = add.astype(BF)
             down_out[t, rows(add_at, h)] = top
@@ -955,7 +978,9 @@
 
     for t in range(early):
         x_copy(t).wait()
-        start_direct(t)
+        start_direct(t, True)
+        if t == 0:
+            start_direct(t, False)
     for load in loads:
         load.start()
     if early < prompts:
@@ -985,9 +1010,9 @@
     fixed[0] = rate
     fixed[1] = bias
     for at in range(n_tp * depth // 128):
-        part = gates_ref[:, at * 128 : (at + 1) * 128].astype(F32)
-        gall[at, pl.ds(0, heads)] = part[:heads]
-        gall[at, pl.ds(heads, heads)] = part[heads:]
+        chunk = gates_ref[:, at * 128 : (at + 1) * 128].astype(F32)
+        gall[at, pl.ds(0, heads)] = chunk[:heads]
+        gall[at, pl.ds(heads, heads)] = chunk[heads:]
         gall[at, pl.ds(2 * heads, pad)] = jnp.zeros((pad, 128), F32)
         picked = [gall[at, pl.ds(tp * nh + k * heads, pad)] for k in range(2)]
         gsel[:, at * 128 : (at + 1) * 128] = jnp.concatenate(picked, axis=0).astype(BF)
@@ -1008,8 +1033,9 @@
 
 
     pass_on(0)
+    start_direct(1, False)
     if early < prompts:
-        start_direct(early)
+        start_direct(early, True)
     for load in loads[6:]:
         load.wait()
     for go in ahead(0):
@@ -1018,9 +1044,13 @@
     def body(t, carry):
         pass_on(t + 1)
 
-        @pl.when(t + 1 + early < prompts)
+        @pl.when(t + 2 < prompts)
         def _():
-            start_direct(t + 1 + early)
+            start_direct(t + 2, False)
+
+        @pl.when(t + 3 < prompts)
+        def _():
+            start_direct(t + 3, True)
 
         gathered(t)
         before(t)
@@ -1093,9 +1123,19 @@
         read_out[:, h * DV : (h + 1) * DV] = read_land[:, h].astype(BF)
 
 
-def close_by(n_sp, n_tp, prompts, seg, rows, nh):
-    even = n_sp >= 2 and n_sp & (n_sp - 1) == 0 and seg & (seg - 1) == 0
-    return even and n_tp == 4 and prompts == n_sp and rows == DK and nh <= 8 and seg >= 8
+def hand_over(state, read, state_out, read_out, sems):
+    pairs = ((state, state_out), (read, read_out))
+    copies = [pltpu.make_async_copy(a, b, sems.at[k]) for k, (a, b) in enumerate(pairs)]
+    for copy in copies:
+        copy.start()
+    for copy in copies:
+        copy.wait()
+
+
+def close_by(n_sp, n_tp, prompts, seg, depth, rows, nh):
+    paired = n_sp >= 4 and n_sp & (n_sp - 1) == 0 and n_tp == 4
+    whole = prompts == n_sp and rows == DK and 1 <= nh <= 8
+    return paired and whole and seg == 128 and depth % 256 == 0
 
 
 def shards(
@@ -1122,9 +1162,9 @@
     smem = pl.BlockSpec(memory_space=pltpu.SMEM)
     hbm = pl.BlockSpec(memory_space=pl.ANY)
     dma = pltpu.SemaphoreType.DMA
-    if close_by(n_sp, n_tp, prompts, seg, rows, nh):
+    if close_by(n_sp, n_tp, prompts, seg, depth, rows, nh):
         hops = n_sp - 1
-        return pl.pallas_call(
+        made = pl.pallas_call(
             functools.partial(near, n_sp, n_tp, nh),
             out_shape=(
                 pltpu.VMEM((rows, nh * DV), BF),
@@ -1183,6 +1223,13 @@
             new_query,
             read_gain.reshape(1, DV),
         )
+        return pl.pallas_call(
+            hand_over,
+            out_shape=tuple(jax.ShapeDtypeStruct(a.shape, a.dtype) for a in made),
+            in_specs=[vmem, vmem],
+            out_specs=(hbm, hbm),
+            scratch_shapes=[dma((2,))],
+        )(*[pltpu.with_memory_space_constraint(a, pltpu.VMEM) for a in made])
     return pl.pallas_call(
         functools.partial(kernel, n_sp, n_tp, nh, rows),
         out_shape=(

time: 52.2 us -> 50.7 us (0.971)
  local copies, waits for them, and re-layouts: 1.26 us -> 0 us
    unnamed x2 -> x0, local copies, waits for them, and re-layouts: 1.26 us -> none
    pallas_call x1, Pallas kernels: 50.2 us -> 49.2 us  [shards(): pl.pallas_call(functools.partial(near, n_sp, n_tp, nh), out_shape=(pltpu....]
    pallas_call x0 -> x1, Pallas kernels: none -> 0.68 us  [shards(): pl.pallas_call(hand_over, out_shape=tuple((jax.ShapeDtypeStruct(a.shape,...]
where the time goes in v3:
time: 50.7 us; the launch traced here: 50.5 us
  Pallas kernels  49.9 us (98%)
  between operations  0.64 us (1%)
    pallas_call x1, Pallas kernels, shards(): pl.pallas_call(functools.partial(near, n_sp, n_tp, nh), out_shape=(pltpu....  49.2 us

profile of v3, /device:TPU:0, one launch (start us, length us, event | category | flops | bytes accessed | tf_op | source)
XLA Modules:
  0.0 50.5 jit_solution(18201082901171296092)
XLA Ops:
  0.6 49.2 %shard_map.104 = (bf16[128,512]{1,0:T(8,128)(2,1)S(1)}, bf16[8,512]{1,0:T(8,128)(2,1)S(1)}) custom-call(bf16[8,128,512]{2,1,0:T(8,128)(2,1)} %x_hbm.1, bf16[2048,512]{1,0:T(8,128)(2,1)} %wk_hbm.1, bf16[2048,512]{1,0:T(8,128)(2,1)} %wv_hbm.1, bf16[32,2048]{1,0:T(8,128)(2,1)} %bitcast.4, f32[4]{0:T(128)} %rate_hbm.1, f32[4]{0:T(128)} %bias_hbm.1, ...), custom_call_target="tpu_custom_call" | custom-call | tf_op jit(solution)/shard_map/pallas_call | solution.py:1167
  49.8 0.7 %shard_map.105 = (bf16[128,512]{1,0:T(8,128)(2,1)}, bf16[8,512]{1,0:T(8,128)(2,1)}) custom-call(bf16[128,512]{1,0:T(8,128)(2,1)S(1)} %get-tuple-element.4.state, bf16[8,512]{1,0:T(8,128)(2,1)S(1)} %get-tuple-element.5.read), custom_call_target="tpu_custom_call" | custom-call | tf_op jit(solution)/shard_map/pallas_call | solution.py:1226

commit v4 on v3

--- a/solution.py
+++ b/solution.py
@@ -769,12 +769,6 @@
         ).T
         lev = level[...]
         strict = lev >= 0
-        eye = jnp.where(
-            lax.broadcasted_iota(jnp.int32, (seg, seg), 0)
-            == lax.broadcasted_iota(jnp.int32, (seg, seg), 1),
-            1.0,
-            0.0,
-        ).astype(F32)
         hs = range(nh)
         keys, grams = [], []
         for h in hs:
@@ -787,56 +781,40 @@
         value_pre = acc[slot, :, width:] + dot(x, weights(late, pl.ds(width, nh * DV)))
         fill()
         fill()
-        lower, inv = [], []
-        for h in hs:
-            spread = cols[:, h : h + 1] - run[h : h + 1, :]
-            low = jnp.where(strict, grams[h] * jnp.exp(jnp.where(strict, spread, 0.0)), 0.0)
-            lower.append(low)
-            inv.append(eye - jnp.where(lev == 0, low, 0.0))
-
-        def merge(first, until):
-            inside = jnp.logical_and(lev >= first, lev < until)
-            cuts = [jnp.where(inside, low, 0.0).astype(BF) for low in lower]
-            return [dot(f.astype(BF), cut).astype(BF) for f, cut in zip(inv, cuts)]
-
-        for first, until in groups[:-1]:
-            steps = merge(first, until)
-            fill()
-            for k in range(first, until - 1):
-                both = [
-                    dot(e, jnp.concatenate([e, f.astype(BF)], axis=1))
-                    for e, f in zip(steps, inv)
-                ]
-                steps = [b[:, :seg].astype(BF) for b in both]
-                fill()
-                inv = [f - b[:, seg:] if k == first else f + b[:, seg:] for f, b in zip(inv, both)]
-            one = until - 1 == first
-            moves = [dot(e, f.astype(BF)) for e, f in zip(steps, inv)]
-            inv = [f - m if one else f + m for f, m in zip(inv, moves)]
         sides = []
         for h in hs:
             pre = value_pre[:, h * DV : (h + 1) * DV]
             value = pre * jax.nn.sigmoid(pre)
-            sides.append(
-                jnp.concatenate(
-                    [
-                        value * cols[:, pad + h : pad + h + 1],
-                        keys[h] * cols[:, 2 * pad + h : 2 * pad + h + 1],
-                    ],
-                    axis=1,
-                )
-            )
-        first, until = groups[-1]
-        steps = merge(first, until)
-        sides = [
-            side + dot((f - eye).astype(BF), side.astype(BF)) for f, side in zip(inv, sides)
-        ]
+            spread = cols[:, h : h + 1] - run[h : h + 1, :]
+            low = jnp.where(strict, grams[h] * jnp.exp(jnp.where(strict, spread, 0.0)), 0.0)
+            cuts = [
+                jnp.where(jnp.logical_and(lev >= first, lev < until), low, 0.0)
+                for first, until in groups
+            ]
+            side = [
+                value * cols[:, pad + h : pad + h + 1],
+                keys[h] * cols[:, 2 * pad + h : 2 * pad + h + 1],
+            ]
+            whole = jnp.concatenate(cuts + side, axis=1)
+            pair = jnp.where(lev == 0, low, 0.0).astype(BF)
+            sides.append(whole - dot(pair, whole.astype(BF)))
         fill()
-        sides = [side - dot(e, side.astype(BF)) for e, side in zip(steps, sides)]
-        for _ in range(first + 1, until):
-            steps = [dot(e, e).astype(BF) for e in steps]
-            fill()
-            sides = [side + dot(e, side.astype(BF)) for e, side in zip(steps, sides)]
+        for first, until in groups:
+            steps = [side[:, :seg].astype(BF) for side in sides]
+            sides = [side[:, seg:] for side in sides]
+            for k in range(first, until):
+                final = k == until - 1
+                given = [side.astype(BF) for side in sides]
+                if not final:
+                    given = [jnp.concatenate([e, g], axis=1) for e, g in zip(steps, given)]
+                made = [dot(e, g) for e, g in zip(steps, given)]
+                if not final:
+                    steps = [m[:, :seg].astype(BF) for m in made]
+                    made = [m[:, seg:] for m in made]
+                sides = [
+                    side - m if k == first else side + m for side, m in zip(sides, made)
+                ]
+                fill()
         while pieces:
             fill()
         tall = ((0,), (0,))
@@ -960,21 +938,42 @@
         dec = later(at) if above else None
         for h in range(nh):
             state = moved(at, sp, h) if below else adds[sp, h]
+            top = state.astype(BF)
+            asked = query[h].astype(BF)
+            if above:
+                turned = dec[h : h + 1] * query[h] - dot(asked, down_in[at, rows(map_at, h)])
+                high = turned.astype(BF).astype(F32)
+                both = jnp.concatenate([high, turned - high], axis=0).astype(BF)
+                terms = dot(both, top)
+                raw = (
+                    terms[:pad]
+                    + terms[pad:]
+                    + dot(asked, down_in[at, rows(add_at, h)])
+                    + dot(asked, down_in[at, rows(low_at, h)])
+                )
+            else:
+                raw = dot(asked, top)
+            norm = (
+                raw
+                * lax.rsqrt(jnp.mean(raw * raw, axis=-1, keepdims=True) + EPS)
+                * gain_ref[...]
+            )
+            read_buf[pl.ds(h, 1)] = norm[:1]
+            if below:
+                adds[sp, h] = state
+
+    def store(above):
+        at = last - 1
+        dec = later(at) if above else None
+        for h in range(nh):
+            state = adds[sp, h]
             if above:
                 state = (
                     dec[h : h + 1] * state
                     + total(at, h)
                     - dot(down_in[at, rows(map_at, h)], state.astype(BF))
                 )
-            cached = state.astype(BF)
-            state_out[:, h * DV : (h + 1) * DV] = cached
-            raw = dot(query[h].astype(BF), cached)
-            norm = (
-                raw
-                * lax.rsqrt(jnp.mean(raw * raw, axis=-1, keepdims=True) + EPS)
-                * gain_ref[...]
-            )
-            read_buf[pl.ds(h, 1)] = norm[:1]
+            state_out[:, h * DV : (h + 1) * DV] = state.astype(BF)
 
     for t in range(early):
         x_copy(t).wait()
@@ -1052,8 +1051,8 @@
         def _():
             start_direct(t + 3, True)
 
+        before(t)
         gathered(t)
-        before(t)
         work(t, ahead(t + 1))
         after(t)
         return carry
@@ -1089,6 +1088,8 @@
 
     lax.fori_loop(1, n_sp, tell, 0)
     read_land[sp] = read_buf[...]
+    pl.when(sp < last)(lambda: store(True))
+    pl.when(sp == last)(lambda: store(False))
 
     block = gath.at[pl.ds(0, n_tp - 1)]
     pltpu.make_async_remote_copy(

time: 50.7 us -> 50.1 us (0.988)
  Pallas kernels: 49.9 us -> 49.3 us
    pallas_call x1, Pallas kernels: 49.2 us -> 48.6 us  [shards(): pl.pallas_call(functools.partial(near, n_sp, n_tp, nh), out_shape=(pltpu....]
where the time goes in v4:
time: 50.1 us; the launch traced here: 50 us
  Pallas kernels  49.3 us (98%)
  between operations  0.64 us (1%)
    pallas_call x1, Pallas kernels, shards(): pl.pallas_call(functools.partial(near, n_sp, n_tp, nh), out_shape=(pltpu....  48.6 us

profile of v4, /device:TPU:0, one launch (start us, length us, event | category | flops | bytes accessed | tf_op | source)
XLA Modules:
  0.0 50.0 jit_solution(14263161885872938847)
XLA Ops:
  0.6 48.6 %shard_map.104 = (bf16[128,512]{1,0:T(8,128)(2,1)S(1)}, bf16[8,512]{1,0:T(8,128)(2,1)S(1)}) custom-call(bf16[8,128,512]{2,1,0:T(8,128)(2,1)} %x_hbm.1, bf16[2048,512]{1,0:T(8,128)(2,1)} %wk_hbm.1, bf16[2048,512]{1,0:T(8,128)(2,1)} %wv_hbm.1, bf16[32,2048]{1,0:T(8,128)(2,1)} %bitcast.4, f32[4]{0:T(128)} %rate_hbm.1, f32[4]{0:T(128)} %bias_hbm.1, ...), custom_call_target="tpu_custom_call" | custom-call | tf_op jit(solution)/shard_map/pallas_call | solution.py:1168
  49.3 0.7 %shard_map.105 = (bf16[128,512]{1,0:T(8,128)(2,1)}, bf16[8,512]{1,0:T(8,128)(2,1)}) custom-call(bf16[128,512]{1,0:T(8,128)(2,1)S(1)} %get-tuple-element.4.state, bf16[8,512]{1,0:T(8,128)(2,1)S(1)} %get-tuple-element.5.read), custom_call_target="tpu_custom_call" | custom-call | tf_op jit(solution)/shard_map/pallas_call | solution.py:1227
